TPU v7x, 256 devices: a whole 4x4x8 slice. The times are simulated.
256 devices in a mesh: kv: 32 (over z, x), tp: 8 (over y, core).
Axes of the slice: x: 4, y: 4, z: 8, core: 2. Of those that a mesh axis runs over, the one named last changes fastest.
Arguments:
- tokens: bfloat16 [256, 4, 4096], P(None, None, 'kv')
- norm_gain: float32 [4096], replicated, may hold values from 0.1 to 1.9
- w_query: bfloat16 [4096, 4096], P('kv', 'tp'), may hold values from -0.09375 to 0.09375
- w_key: bfloat16 [4096, 4096], P('kv', 'tp'), may hold values from -0.09375 to 0.09375
- w_value: bfloat16 [4096, 4096], P('kv', 'tp'), may hold values from -0.09375 to 0.09375
- w_gate: bfloat16 [4096, 4096], P('kv', 'tp'), may hold values from -0.09375 to 0.09375
- w_decay: bfloat16 [4096, 32], replicated, may hold values from -0.09375 to 0.09375
- w_beta: bfloat16 [4096, 32], replicated, may hold values from -0.09375 to 0.09375
- decay_rate: float32 [32], replicated, may hold values from 0.02 to 3
- head_gain: float32 [128], replicated, may hold values from 0.1 to 1.9
- w_out: bfloat16 [4096, 4096], P('tp', 'kv'), may hold values from -0.09375 to 0.09375
- state: float32 [256, 32, 128, 128], P('kv', 'tp'), may hold values from -0.4 to 0.4
- prev_keys: bfloat16 [256, 32, 4, 128], P('kv', 'tp'), may hold values from -6 to 6
- prev_values: bfloat16 [256, 32, 4, 128], P('kv', 'tp'), may hold values from -6 to 6
- prev_log_decay: float32 [256, 32, 4], P('kv', 'tp'), may hold values from -0.7 to -0.02
- prev_beta: float32 [256, 32, 4], P('kv', 'tp'), may hold values from 0.1 to 0.9
- accepted: int32 [256], P('kv'), may hold values from 0 to 4
Outputs:
- mixed: bfloat16 [256, 4, 4096], P('tp', None, 'kv')
- carried: float32 [256, 32, 128, 128], P('kv', 'tp')
All inputs are finite; a program needn't handle non-finite values.
Results may differ from a plain program's by a relative error of at most 0.0069.
Values may be sent and summed in bfloat16 or wider, within the bound.
No kernel may reach another device: no remote copies, remote signals or barrier semaphores. Data moves between devices by JAX's collectives and lax.ppermute only.
A program may use at most 128 MiB of HBM per device.

v0:
```python
import jax
import jax.numpy as jnp
from jax import lax
from jax.experimental import pallas as pl
from jax.experimental.pallas import tpu as pltpu
from jax.sharding import Mesh
from jax.sharding import PartitionSpec as P

epsilon = 1e-06
ZS, XS, TP = (8, 4, 8)
PROPS = 4
SEQ = 8
HEADS = 4
DK = 128
ROWS = SEQ * PROPS
GROUP = ZS * ROWS
COLS = HEADS * DK
WIDE = 4 * COLS + 128
FOLD = ZS // 2 + 1
f32 = jnp.float32
bf16 = jnp.bfloat16


VMEM = pl.BlockSpec(memory_space=pltpu.VMEM)
ANY = pl.BlockSpec(memory_space=pl.ANY)
SMEM = pl.BlockSpec(memory_space=pltpu.SMEM)


def ring(step, size):
    return [(i, (i + step) % size) for i in range(size)]


def hidot(a, b):
    return lax.dot_general(
        a, b, (((1,), (0,)), ((), ())), precision=lax.Precision.HIGHEST, preferred_element_type=f32
    )


def spread(rows, matrix_count):
    which = lax.broadcasted_iota(jnp.int32, rows.shape, 0) % matrix_count
    return jnp.concatenate([jnp.where(which == j, rows, 0.0) for j in range(matrix_count)], axis=1)


def lane_sum(a):
    return jnp.sum(a, axis=-1, keepdims=True)


def slab(a, t):
    return a[t * SEQ : (t + 1) * SEQ]


def decays(logs):
    table = {}
    for s in range(-1, PROPS):
        total = None
        for t in range(s + 1, PROPS):
            total = logs[t] if total is None else total + logs[t]
            table[s, t] = jnp.exp(total)
        table[s, s] = None
    return table


def writes(keys, values, strength, decay, read):
    done = []
    for t in range(PROPS):
        predicted = decay[-1, t] * read[t]
        for s in range(t):
            predicted = predicted + (decay[s, t] * lane_sum(keys[s] * keys[t])) * done[s]
        done.append(strength[t] * (values[t] - predicted))
    return done


def head_copies(outer, inner, sems, inward):
    pairs = [(outer.at[:, h], inner.at[h]) for h in range(HEADS)]
    return [
        pltpu.make_async_copy(*(pair if inward else pair[::-1]), sems.at[h]) for h, pair in enumerate(pairs)
    ]


def carried_kernel(state_ref, keys_ref, values_ref, logs_ref, beta_ref, out_ref, old_ref, new_ref, sems):
    loads = head_copies(state_ref, old_ref, sems.at[0], True)
    stores = head_copies(out_ref, new_ref, sems.at[1], False)
    for load in loads:
        load.start()
    lane = lax.broadcasted_iota(jnp.int32, (DK, ROWS), 1) % SEQ
    for h in range(HEADS):
        raw = keys_ref[h]
        unit = raw * lax.rsqrt(lane_sum(raw * raw) + epsilon)
        vals = values_ref[h]
        loads[h].wait()
        matrix = old_ref[h].reshape(SEQ * DK, DK)
        read = hidot(spread(unit, SEQ), matrix)
        keys = [slab(unit, t) for t in range(PROPS)]
        col = lambda ref, t: ref[:, h * PROPS + t : h * PROPS + t + 1]
        logs = [col(logs_ref, t) for t in range(PROPS)]
        strength = [col(beta_ref, t) for t in range(PROPS)]
        decay = decays(logs)
        done = writes(
            keys, [slab(vals, t) for t in range(PROPS)], strength, decay, [slab(read, t) for t in range(PROPS)]
        )
        last = PROPS - 1
        scaled = [keys[t] if t == last else decay[t, last] * keys[t] for t in range(PROPS)]
        kcols = jnp.concatenate(scaled, axis=0).T
        urows = jnp.concatenate(done, axis=0)
        for j in range(SEQ):
            step = hidot(jnp.where(lane == j, kcols, 0.0), urows)
            keep = decay[-1, last][j : j + 1, :]
            new_ref[h, j] = keep * old_ref[h, j] + step
        stores[h].start()
    for store in stores:
        store.wait()


def squares_kernel(tok_ref, out_ref):
    total = jnp.zeros((GROUP, 128), f32)
    for s in range(XS):
        feats = tok_ref[s].astype(f32)
        total = total + feats * feats
    ones = jnp.ones((8, 128), f32)
    rows = lax.dot_general(
        ones, total, (((1,), (1,)), ((), ())), precision=lax.Precision.HIGHEST, preferred_element_type=f32
    )
    for s in range(ZS):
        out_ref[s] = rows[0:1]


def columns_kernel(place_ref, tok_ref, squares_ref, gain_ref, ab_ref, *refs):
    pieces, (own_ref, *block_refs, norm_ref, scale_ref) = (refs[: 2 * XS], refs[2 * XS :])
    z, x = (place_ref[0], place_ref[1])
    squares = squares_ref[0]
    for s in range(1, ZS):
        squares = squares + squares_ref[s]
    scale = lax.rsqrt(squares / 4096 + epsilon)
    scale_ref[...] = jnp.broadcast_to(scale, (128, GROUP)).T
    extra = jnp.zeros((GROUP, 16), f32)
    for r in range(XS):
        at = lax.rem(x + XS - r, XS)
        for d in range(ZS):
            rows = pl.ds(pl.multiple_of(lax.rem(z + d, ZS) * ROWS, ROWS), ROWS)
            feats = tok_ref[at, rows, :].astype(f32)
            piece = (feats * scale_ref[rows, :] * gain_ref[at]).astype(bf16)
            norm_ref[d * ROWS : (d + 1) * ROWS, r * 128 : (r + 1) * 128] = piece
        extra = extra + lax.dot_general(
            norm_ref[:, r * 128 : (r + 1) * 128],
            ab_ref[at],
            (((1,), (1,)), ((), ())),
            preferred_element_type=f32,
        )
    normed = norm_ref[...]

    def put(lo, hi, part):
        for d in range(ZS):
            rows = part[d * ROWS : (d + 1) * ROWS]
            if d == 0:
                own_ref[:, lo:hi] = rows
            else:
                ref = block_refs[d - 1]
                ref[:, lo:hi] = rows.astype(ref.dtype)

    for pair in range(2):
        mine = pieces[pair * XS : (pair + 1) * XS]
        for half in range(2):
            weight = jnp.concatenate([w[half * 128 : (half + 1) * 128, :] for w in mine], axis=0)
            at = (2 * pair + half) * COLS
            put(at, at + COLS, jnp.dot(normed, weight, preferred_element_type=f32))
    zero = jnp.zeros((GROUP, 112), f32)
    put(4 * COLS, WIDE, jnp.concatenate([extra, zero], axis=1))
    low = extra - extra.astype(bf16).astype(f32)
    for d in range(1, ZS):
        if d != FOLD:
            rows = low[d * ROWS : (d + 1) * ROWS]
            block_refs[d - 1][:, 4 * COLS + 16 : 4 * COLS + 32] = rows.astype(bf16)


def fold_kernel(came_ref, own_ref, out_ref):
    total = came_ref[...].astype(f32) + own_ref[...]
    out_ref[...] = total.astype(bf16)
    at = 4 * COLS
    extra = total[:, at : at + 16] + total[:, at + 16 : at + 32]
    high = extra.astype(bf16)
    out_ref[:, at : at + 16] = high
    out_ref[:, at + 16 : at + 32] = (extra - high.astype(f32)).astype(bf16)


def unit(a):
    return a * lax.rsqrt(lane_sum(a * a) + epsilon)


def silu(a):
    return a * jax.nn.sigmoid(a)


def attend_kernel(rate_ref, carried_ref, gain_ref, own_ref, *refs):
    came, (out_ref, rows_ref, heads_ref) = (refs[:-3], refs[-3:])

    def total(lo, hi):
        acc = own_ref[:, lo:hi]
        for ref in came:
            acc = acc + ref[:, lo:hi].astype(f32)
        return acc

    def regroup(index, rows):
        rows_ref[index] = rows
        return jnp.concatenate(
            [rows_ref[index, pl.ds(t, SEQ, stride=PROPS), :] for t in range(PROPS)], axis=0
        )

    extra = regroup(0, total(4 * COLS, WIDE))
    for h in range(HEADS):
        lo, hi = (h * DK, (h + 1) * DK)
        spot = 1 + 4 * h
        query = unit(silu(regroup(spot, total(lo, hi)))) * DK ** (-0.5)
        key = unit(silu(regroup(spot + 1, total(COLS + lo, COLS + hi))))
        value = silu(regroup(spot + 2, total(2 * COLS + lo, 2 * COLS + hi)))
        gate = silu(regroup(spot + 3, total(3 * COLS + lo, 3 * COLS + hi)))
        araw = extra[:, h : h + 1] + extra[:, 16 + h : 17 + h]
        braw = extra[:, 4 + h : 5 + h] + extra[:, 20 + h : 21 + h]
        strength = jax.nn.sigmoid(braw)
        soft = jnp.maximum(araw, 0.0) + jnp.log1p(jnp.exp(-jnp.abs(araw)))
        log = -rate_ref[h] * soft
        matrix = carried_ref[:, h].reshape(SEQ * DK, DK)
        read = hidot(spread(jnp.concatenate([key, query], axis=0), SEQ), matrix)
        keys = [slab(key, t) for t in range(PROPS)]
        decay = decays([slab(log, t) for t in range(PROPS)])
        done = writes(
            keys,
            [slab(value, t) for t in range(PROPS)],
            [slab(strength, t) for t in range(PROPS)],
            decay,
            [slab(read, t) for t in range(PROPS)],
        )
        for t in range(PROPS):
            q = slab(query, t)
            att = decay[-1, t] * slab(read, PROPS + t)
            for s in range(t + 1):
                weight = lane_sum(keys[s] * q)
                if s < t:
                    weight = decay[s, t] * weight
                att = att + weight * done[s]
            att = att * lax.rsqrt(jnp.mean(att * att, axis=-1, keepdims=True) + epsilon)
            heads_ref[h, pl.ds(t, SEQ, stride=PROPS), :] = att * gain_ref[...] * slab(gate, t)
        head = heads_ref[h].astype(bf16)
        for s in range(ZS):
            out_ref[s, :, lo:hi] = head


def project_kernel(x_ref, heads_ref, w0, w1, w2, w3, out_ref):
    x = x_ref[0]
    rows = heads_ref[...].reshape(GROUP, COLS)
    for r, w in enumerate((w0, w1, w2, w3)):
        at = lax.rem(x + XS - r, XS)
        part = jnp.dot(rows, w[...], preferred_element_type=f32).astype(bf16)
        out_ref[pl.ds(at * TP, TP)] = part.reshape(TP, ROWS, 128)


def final_kernel(terms_ref, out_ref):
    for s in range(XS):
        total = terms_ref[s * TP].astype(f32)
        for t in range(1, TP):
            total = total + terms_ref[s * TP + t].astype(f32)
        out_ref[pl.ds(s * ROWS, ROWS), :] = total.astype(bf16)


def call(kernel, out, specs, flops, scratch=(), grant=16384, placed=VMEM):
    return pl.pallas_call(
        kernel,
        out_shape=out,
        in_specs=specs,
        out_specs=jax.tree.map(lambda _: placed, out),
        scratch_shapes=scratch,
        compiler_params=pltpu.CompilerParams(vmem_limit_bytes=grant * 1024),
        cost_estimate=pl.CostEstimate(flops=flops, bytes_accessed=1 << 20, transcendentals=0),
    )


def shift(shard, step, axis="x"):
    return lax.ppermute(shard, axis, ring(step, lax.axis_size(axis)))


def exchange(blocks, axes):
    return lax.all_to_all(blocks, axes, 0, 0, tiled=True)


def step(
    tokens,
    norm_gain,
    w_query,
    w_key,
    w_value,
    w_gate,
    w_decay,
    w_beta,
    decay_rate,
    head_gain,
    w_out,
    state,
    prev_keys,
    prev_values,
    prev_log_decay,
    prev_beta,
    accepted,
):
    z = lax.axis_index("z")
    x = lax.axis_index("x")
    tp = lax.axis_index("tp")
    shape = jax.ShapeDtypeStruct
    xs = x.astype(jnp.int32).reshape(1)

    blocks = tokens.reshape(ZS, XS, ROWS, 128).transpose(1, 0, 2, 3).reshape(XS, GROUP, 128)
    tok = exchange(blocks, "x")

    w_qk = jnp.concatenate([w_query, w_key], axis=0)
    w_vz = jnp.concatenate([w_value, w_gate], axis=0)
    qk1 = shift(w_qk, 1)
    vz3 = shift(w_vz, -1)
    vz1 = shift(w_vz, 1)
    qk3 = shift(w_qk, -1)
    qk2 = shift(qk1, 1)
    vz2 = shift(vz3, -1)

    squares = call(squares_kernel, shape((ZS, 1, GROUP), f32), [VMEM], 1 << 20)(tok)
    squares = exchange(squares, "z")
    gain = lax.dynamic_slice_in_dim(norm_gain, z * 512, 512, 0).reshape(XS, 1, 128)
    ab = jnp.concatenate(
        [
            lax.dynamic_slice(w.T, (tp * HEADS, z * 512), (HEADS, 512)).reshape(HEADS, XS, 128)
            for w in (w_decay, w_beta)
        ]
        + [jnp.zeros((8, XS, 128), bf16)],
        axis=0,
    ).transpose(1, 0, 2)

    types = [f32 if d in (0, FOLD) else bf16 for d in range(ZS)]
    own, *block = call(
        columns_kernel,
        [shape((ROWS, WIDE), t) for t in types],
        [SMEM] + [VMEM] * 12,
        2 * GROUP * 512 * 2048,
        [pltpu.VMEM((GROUP, 512), bf16), pltpu.VMEM((GROUP, 128), f32)],
    )(jnp.stack([z, x]).astype(jnp.int32), tok, squares, gain, ab, w_qk, qk1, qk2, qk3, w_vz, vz1, vz2, vz3)
    came = {4: shift(block[3], -1, "z")}
    for d in (3, 2, 6, 1, 7):
        came[d] = shift(block[d - 1], d, "z")
    folded = call(fold_kernel, shape((ROWS, WIDE), bf16), [VMEM] * 2, 1 << 20)(came.pop(4), block[4])
    came[5] = shift(folded, 5, "z")

    o1 = shift(w_out, 1)
    o3 = shift(w_out, -1)
    o2 = shift(o1, 1)

    keep = (jnp.arange(PROPS)[None, :] < accepted[:, None]).astype(f32)[:, None, :]
    logs = (prev_log_decay * keep).reshape(SEQ, HEADS * PROPS)
    strengths = (prev_beta * keep).reshape(SEQ, HEADS * PROPS)
    old_keys = prev_keys.astype(f32).transpose(1, 2, 0, 3).reshape(HEADS, ROWS, DK)
    old_values = prev_values.astype(f32).transpose(1, 2, 0, 3).reshape(HEADS, ROWS, DK)
    whole = shape(state.shape, f32)
    buffer = pltpu.VMEM((HEADS, SEQ, DK, DK), f32)
    carried = call(
        carried_kernel,
        whole,
        [ANY] + [VMEM] * 4,
        1 << 31,
        [buffer, buffer, pltpu.SemaphoreType.DMA((2, HEADS))],
        60 * 1024,
        ANY,
    )(state, old_keys, old_values, logs, strengths)

    rate = lax.dynamic_slice_in_dim(decay_rate, tp * HEADS, HEADS, 0)
    heads = call(
        attend_kernel,
        shape((ZS, ROWS, COLS), bf16),
        [SMEM] + [VMEM] * 9,
        1 << 30,
        [
            pltpu.VMEM((1 + 4 * HEADS, ROWS, DK), f32),
            pltpu.VMEM((HEADS, ROWS, DK), f32),
        ],
    )(rate, carried, head_gain.reshape(1, 128), own, *came.values())
    heads = exchange(heads, "z")
    terms = call(
        project_kernel,
        shape((XS * TP, ROWS, 128), bf16),
        [SMEM] + [VMEM] * 5,
        2 * GROUP * 512 * 512,
    )(xs, heads, w_out, o1, o2, o3)
    terms = exchange(terms, ("x", "tp"))
    mixed = call(final_kernel, shape((XS * ROWS, 128), bf16), [VMEM], 1 << 20)(terms)
    return (mixed.reshape(XS * SEQ, PROPS, 128), carried)


def solution(mesh):
    grid = Mesh(mesh.devices.reshape(ZS, XS, TP), ("z", "x", "tp"))
    kv = ("z", "x")
    placed = (
        P(None, None, kv),
        P(),
        P(kv, "tp"),
        P(kv, "tp"),
        P(kv, "tp"),
        P(kv, "tp"),
        P(),
        P(),
        P(),
        P(),
        P("tp", kv),
        P(kv, "tp", None, None),
        P(kv, "tp", None, None),
        P(kv, "tp", None, None),
        P(kv, "tp", None),
        P(kv, "tp", None),
        P(kv),
    )
    return jax.shard_map(
        step,
        mesh=grid,
        in_specs=placed,
        out_specs=(P("tp", None, kv), P(kv, "tp", None, None)),
        check_vma=False,
    )
```

profile of v0, /device:TPU:1, one launch (start us, length us, event | category | flops | bytes accessed | tf_op | source)
XLA Modules:
  0.0 101.4 jit_solution(6201973893855360926)
XLA Ops:
  0.7 0.9 constant_dynamic-update-slice_fusion.1
  1.6 0.9 constant_dynamic-update-slice_fusion.refs_0_
  2.6 2.1 %collective-permute-start = (bf16[256,512]{1,0:T(8,128)(2,1)S(1)}, bf16[256,512]{1,0:T(8,128)(2,1)S(1)}, u32[]{:S(2)}, u32[]{:S(2)}) collective-permute-start(bf16[256,512]{1,0:T(8,128)(2,1)S(1)} %constant_dynamic-update-slice_fusion.refs_0_), channel_id=1, source_target_pairs={{0,8},{8,16},{16,24},{24,0},{1,9},{9,17},{17,25},{25,1},{2,10},{10... | collective-permute-start | bytes 786440 | tf_op jit(solution)/shard_map/ppermute | solution.py:277
  4.7 1.4 %collective-permute-start.2 = (bf16[256,512]{1,0:T(8,128)(2,1)S(1)}, bf16[256,512]{1,0:T(8,128)(2,1)S(1)}, u32[]{:S(2)}, u32[]{:S(2)}) collective-permute-start(bf16[256,512]{1,0:T(8,128)(2,1)S(1)} %constant_dynamic-update-slice_fusion.refs_0_), channel_id=1, source_target_pairs={{0,24},{8,0},{16,8},{24,16},{1,25},{9,1},{17,9},{25,17},{2,26},{10... | collective-permute-start | bytes 786440 | tf_op jit(solution)/shard_map/ppermute | solution.py:277
  6.0 0.9 constant_dynamic-update-slice_fusion.3
  6.9 0.9 constant_dynamic-update-slice_fusion.2.refs_4_
  7.9 1.5 %collective-permute-start.4 = (bf16[256,512]{1,0:T(8,128)(2,1)S(1)}, bf16[256,512]{1,0:T(8,128)(2,1)S(1)}, u32[]{:S(2)}, u32[]{:S(2)}) collective-permute-start(bf16[256,512]{1,0:T(8,128)(2,1)S(1)} %constant_dynamic-update-slice_fusion.2.refs_4_), channel_id=1, source_target_pairs={{0,24},{8,0},{16,8},{24,16},{1,25},{9,1},{17,9},{25,17},{2,26},{10... | collective-permute-start | bytes 786440 | tf_op jit(solution)/shard_map/ppermute | solution.py:277
  9.4 1.7 %copy.23 = bf16[8,4,32,128]{3,2,0,1:T(8,128)(2,1)} copy(bf16[8,4,32,128]{3,2,1,0:T(8,128)(2,1)} %bitcast.36) | data formatting | bytes 524288 | tf_op jit(solution)/shard_map/reshape | solution.py:309
  11.1 3.9 %all-to-all-start = ((bf16[4,256,128]{2,1,0:T(8,128)(2,1)}), bf16[4,256,128]{2,1,0:T(8,128)(2,1)S(1)}, u32[]{:S(2)}, u32[]{:S(2)}) async-start(bf16[4,256,128]{2,1,0:T(8,128)(2,1)} %bitcast.11), calls=%async_computation | async-start | bytes 524288 | tf_op jit(solution)/shard_map/all_to_all | solution.py:281
  15.0 0.8 dynamic-slice_bitcast_fusion
  15.9 1.5 %collective-permute-start.1 = (bf16[256,512]{1,0:T(8,128)(2,1)S(1)}, bf16[256,512]{1,0:T(8,128)(2,1)S(1)}, u32[]{:S(2)}, u32[]{:S(2)}) collective-permute-start(bf16[256,512]{1,0:T(8,128)(2,1)S(1)} %collective-permute-done.refs_1_), channel_id=1, source_target_pairs={{0,8},{8,16},{16,24},{24,0},{1,9},{9,17},{17,25},{25,1},{2,10},{10... | collective-permute-start | bytes 786440 | tf_op jit(solution)/shard_map/ppermute | solution.py:277
  17.5 1.4 %collective-permute-start.5 = (bf16[256,512]{1,0:T(8,128)(2,1)S(1)}, bf16[256,512]{1,0:T(8,128)(2,1)S(1)}, u32[]{:S(2)}, u32[]{:S(2)}) collective-permute-start(bf16[256,512]{1,0:T(8,128)(2,1)S(1)} %collective-permute-done.4.refs_7_), channel_id=1, source_target_pairs={{0,24},{8,0},{16,8},{24,16},{1,25},{9,1},{17,9},{25,17},{2,26},{10... | collective-permute-start | bytes 786440 | tf_op jit(solution)/shard_map/ppermute | solution.py:277
  18.9 1.9 %all-to-all-done.tok_ref = bf16[4,256,128]{2,1,0:T(8,128)(2,1)S(1)} async-done(((bf16[4,256,128]{2,1,0:T(8,128)(2,1)}), bf16[4,256,128]{2,1,0:T(8,128)(2,1)S(1)}, u32[]{:S(2)}, u32[]{:S(2)}) %all-to-all-start) | async-done | bytes 262176 | tf_op jit(solution)/shard_map/all_to_all | solution.py:281
  20.8 0.8 shard_map.177
  21.7 8.2 %all-to-all-start.1 = ((f32[8,1,256]{2,1,0:T(1,128)}), f32[8,1,256]{2,1,0:T(1,128)S(1)}, u32[]{:S(2)}, u32[]{:S(2)}) async-start(f32[8,1,256]{2,1,0:T(1,128)} %shard_map.177), calls=%async_computation.1 | async-start | bytes 16384 | tf_op jit(solution)/shard_map/all_to_all | solution.py:281
  32.1 4.3 %all-to-all-done.1.squares_ref = f32[8,1,256]{2,1,0:T(1,128)S(1)} async-done(((f32[8,1,256]{2,1,0:T(1,128)}), f32[8,1,256]{2,1,0:T(1,128)S(1)}, u32[]{:S(2)}, u32[]{:S(2)}) %all-to-all-start.1) | async-done | bytes 8224 | tf_op jit(solution)/shard_map/all_to_all | solution.py:281
  36.4 1.5 %shard_map.178 = (f32[32,2176]{1,0:T(8,128)S(1)}, bf16[32,2176]{1,0:T(8,128)(2,1)S(1)}, bf16[32,2176]{1,0:T(8,128)(2,1)S(1)}, bf16[32,2176]{1,0:T(8,128)(2,1)S(1...) custom-call(s32[2]{0:T(128)S(1)} %pad_add_fusion.place_ref, ...), custom_call_target="tpu_custom_call" | custom-call | flops 536870912 | bytes 1048576 | tf_op jit(solution)/shard_map/pallas_call | solution.py:334
  39.3 2.1 %collective-permute-start.6 = (bf16[32,2176]{1,0:T(8,128)(2,1)S(1)}, bf16[32,2176]{1,0:T(8,128)(2,1)S(1)}, u32[]{:S(2)}, u32[]{:S(2)}) collective-permute-start(bf16[32,2176]{1,0:T(8,128)(2,1)S(1)} %get-tuple-element.11), channel_id=1, source_target_pairs={{0,96},{32,128},{64,160},{96,192},{128,224},{160,0},{192,32},{224,... | collective-permute-start | bytes 417800 | tf_op jit(solution)/shard_map/ppermute | solution.py:277
  41.4 1.5 %collective-permute-start.7 = (bf16[32,2176]{1,0:T(8,128)(2,1)S(1)}, bf16[32,2176]{1,0:T(8,128)(2,1)S(1)}, u32[]{:S(2)}, u32[]{:S(2)}) collective-permute-start(bf16[32,2176]{1,0:T(8,128)(2,1)S(1)} %get-tuple-element.12), channel_id=1, source_target_pairs={{0,64},{32,96},{64,128},{96,160},{128,192},{160,224},{192,0},{224,... | collective-permute-start | bytes 417800 | tf_op jit(solution)/shard_map/ppermute | solution.py:277
  42.9 2.1 %collective-permute-start.8 = (bf16[32,2176]{1,0:T(8,128)(2,1)S(1)}, bf16[32,2176]{1,0:T(8,128)(2,1)S(1)}, u32[]{:S(2)}, u32[]{:S(2)}) collective-permute-start(bf16[32,2176]{1,0:T(8,128)(2,1)S(1)} %get-tuple-element.13), channel_id=1, source_target_pairs={{0,192},{32,224},{64,0},{96,32},{128,64},{160,96},{192,128},{224,1... | collective-permute-start | bytes 417800 | tf_op jit(solution)/shard_map/ppermute | solution.py:277
  44.9 1.5 %collective-permute-start.9 = (bf16[32,2176]{1,0:T(8,128)(2,1)S(1)}, bf16[32,2176]{1,0:T(8,128)(2,1)S(1)}, u32[]{:S(2)}, u32[]{:S(2)}) collective-permute-start(bf16[32,2176]{1,0:T(8,128)(2,1)S(1)} %get-tuple-element.14), channel_id=1, source_target_pairs={{0,32},{32,64},{64,96},{96,128},{128,160},{160,192},{192,224},{224... | collective-permute-start | bytes 417800 | tf_op jit(solution)/shard_map/ppermute | solution.py:277
  46.6 1.1 %collective-permute-start.12 = (bf16[32,2176]{1,0:T(8,128)(2,1)S(1)}, bf16[32,2176]{1,0:T(8,128)(2,1)S(1)}, u32[]{:S(2)}, u32[]{:S(2)}) collective-permute-start(bf16[32,2176]{1,0:T(8,128)(2,1)S(1)} %shard_map.179), channel_id=1, source_target_pairs={{0,160},{32,192},{64,224},{96,0},{128,32},{160,64},{192,96},{224,1... | collective-permute-start | bytes 417800 | tf_op jit(solution)/shard_map/ppermute | solution.py:277
  47.7 6.5 %shard_map.176.carried_ref = f32[8,4,128,128]{3,2,1,0:T(8,128)} custom-call(f32[8,4,128,128]{3,2,1,0:T(8,128)} %state_ref.1, f32[4,32,128]{2,1,0:T(8,128)} %get-tuple-element.23.keys_ref, f32[4,32,128]{2,1,0:T(8,128)} %get-tuple-element.22.values_ref, f32[8,16]{1,0:T(8,128)} %copy.21.logs_ref, f32[8,16]{1,0:T(8,128)} %copy.22.beta_ref), custom_call_target="tpu_custom_call" | custom-call | flops 2147483648 | bytes 1048576 | tf_op jit(solution)/shard_map/pallas_call | solution.py:358
  54.3 6.0 %collective-permute-done.9.refs_3_ = bf16[32,2176]{1,0:T(8,128)(2,1)S(1)} collective-permute-done((bf16[32,2176]{1,0:T(8,128)(2,1)S(1)}, bf16[32,2176]{1,0:T(8,128)(2,1)S(1)}, u32[]{:S(2)}, u32[]{:S(2)}) %collective-permute-start.9) | collective-permute-done | bytes 139296 | tf_op jit(solution)/shard_map/ppermute | solution.py:277
  60.3 1.6 %copy-done.2 = f32[8,4,128,128]{3,2,1,0:T(8,128)S(1)} copy-done((f32[8,4,128,128]{3,2,1,0:T(8,128)S(1)}, f32[8,4,128,128]{3,2,1,0:T(8,128)}, u32[]{:S(2)}) %copy-start.2) | copy-done | bytes 2097176
  61.9 3.0 %shard_map.180 = bf16[8,32,512]{2,1,0:T(8,128)(2,1)} custom-call(f32[4]{0:T(128)S(1)} %dynamic_slice.12.rate_ref, f32[8,4,128,128]{3,2,1,0:T(8,128)S(1)} %copy-done.2, f32[1,128]{1,0:T(1,128)S(1)} %bitcast.35, f32[32,2176]{1,0:T(8,128)S(1)} %get-tuple-element.10.own_ref, bf16[32,2176]{1,0:T(8,128)(2,1)S(1)} %collective-permute-done.6.refs_0_, ...), custom_call_target="tpu_custom_call" | custom-call | flops 1073741824 | bytes 1048576 | tf_op jit(solution)/shard_map/pallas_call | solution.py:369
  64.9 3.4 %all-to-all-start.2 = ((bf16[8,32,512]{2,1,0:T(8,128)(2,1)}), bf16[8,32,512]{2,1,0:T(8,128)(2,1)S(1)}, u32[]{:S(2)}, u32[]{:S(2)}) async-start(bf16[8,32,512]{2,1,0:T(8,128)(2,1)} %shard_map.180), calls=%async_computation.2 | async-start | bytes 524288 | tf_op jit(solution)/shard_map/all_to_all | solution.py:281
  68.3 1.2 %collective-permute-start.13 = (bf16[512,128]{1,0:T(8,128)(2,1)S(1)}, bf16[512,128]{1,0:T(8,128)(2,1)S(1)}, u32[]{:S(2)}, u32[]{:S(2)}) collective-permute-start(bf16[512,128]{1,0:T(8,128)(2,1)S(1)} %copy-done), channel_id=1, source_target_pairs={{0,8},{8,16},{16,24},{24,0},{1,9},{9,17},{17,25},{25,1},{2,10},{10... | collective-permute-start | bytes 393224 | tf_op jit(solution)/shard_map/ppermute | solution.py:277
  69.6 1.5 %collective-permute-start.15 = (bf16[512,128]{1,0:T(8,128)(2,1)S(1)}, bf16[512,128]{1,0:T(8,128)(2,1)S(1)}, u32[]{:S(2)}, u32[]{:S(2)}) collective-permute-start(bf16[512,128]{1,0:T(8,128)(2,1)S(1)} %copy-done), channel_id=1, source_target_pairs={{0,24},{8,0},{16,8},{24,16},{1,25},{9,1},{17,9},{25,17},{2,26},{10... | collective-permute-start | bytes 393224 | tf_op jit(solution)/shard_map/ppermute | solution.py:277
  71.1 2.4 %collective-permute-done.13.w1 = bf16[512,128]{1,0:T(8,128)(2,1)S(1)} collective-permute-done((bf16[512,128]{1,0:T(8,128)(2,1)S(1)}, bf16[512,128]{1,0:T(8,128)(2,1)S(1)}, u32[]{:S(2)}, u32[]{:S(2)}) %collective-permute-start.13) | collective-permute-done | bytes 131104 | tf_op jit(solution)/shard_map/ppermute | solution.py:277
  73.4 5.0 %collective-permute-done.14.w2 = bf16[512,128]{1,0:T(8,128)(2,1)S(1)} collective-permute-done((bf16[512,128]{1,0:T(8,128)(2,1)S(1)}, bf16[512,128]{1,0:T(8,128)(2,1)S(1)}, u32[]{:S(2)}, u32[]{:S(2)}) %collective-permute-start.14) | collective-permute-done | bytes 131104 | tf_op jit(solution)/shard_map/ppermute | solution.py:277
  78.9 21.8 %all_to_all.20.terms_ref = bf16[32,32,128]{2,1,0:T(8,128)(2,1)S(1)} all-to-all(bf16[32,32,128]{2,1,0:T(8,128)(2,1)S(1)} %shard_map.181), channel_id=1, replica_groups=mesh['z'=8,'x'=4,'tp'=8] {'x','tp'}, dimensions={0} | all-to-all | bytes 524288 | tf_op jit(solution)/shard_map/all_to_all | solution.py:281
  (52 shorter events, 5.2 us)
Async XLA Ops:
  0.6 14.3 %copy-start.3 = (bf16[8,4,4,128]{3,2,1,0:T(4,128)(2,1)S(1)}, bf16[8,4,4,128]{3,2,1,0:T(4,128)(2,1)}, u32[]{:S(2)}) copy-start(bf16[8,4,4,128]{3,2,1,0:T(4,128)(2,1)} %param.30) | copy-start | bytes 98308
  0.6 14.3 %copy-start.7 = (s32[8]{0:T(128)S(1)}, s32[8]{0:T(128)}, u32[]{:S(2)}) copy-start(s32[8]{0:T(128)} %param.33) | copy-start | bytes 100
  0.7 14.3 %copy-start.5 = (f32[8,4,4]{0,2,1:T(4,128)S(1)}, f32[8,4,4]{0,2,1:T(4,128)}, u32[]{:S(2)}) copy-start(f32[8,4,4]{0,2,1:T(4,128)} %param.32) | copy-start | bytes 1540
  0.7 14.3 %copy-start.6 = (f32[8,4,4]{0,2,1:T(4,128)S(1)}, f32[8,4,4]{0,2,1:T(4,128)}, u32[]{:S(2)}) copy-start(f32[8,4,4]{0,2,1:T(4,128)} %param.31) | copy-start | bytes 1540
  0.7 15.2 %copy-start.4 = (bf16[8,4,4,128]{3,2,1,0:T(4,128)(2,1)S(1)}, bf16[8,4,4,128]{3,2,1,0:T(4,128)(2,1)}, u32[]{:S(2)}) copy-start(bf16[8,4,4,128]{3,2,1,0:T(4,128)(2,1)} %param.29) | copy-start | bytes 98308
  0.7 30.0 %copy-start.8 = (f32[32]{0:T(128)S(1)}, f32[32]{0:T(128)}, u32[]{:S(2)}) copy-start(f32[32]{0:T(128)} %param.25) | copy-start | bytes 388
  2.6 13.4 %collective-permute-start = (bf16[256,512]{1,0:T(8,128)(2,1)S(1)}, bf16[256,512]{1,0:T(8,128)(2,1)S(1)}, u32[]{:S(2)}, u32[]{:S(2)}) collective-permute-start(bf16[256,512]{1,0:T(8,128)(2,1)S(1)} %constant_dynamic-update-slice_fusion.refs_0_), channel_id=1, source_target_pairs={{0,8},{8,16},{16,24},{24,0},{1,9},{9,17},{17,25},{25,1},{2,10},{10... | collective-permute-start | bytes 786440 | tf_op jit(solution)/shard_map/ppermute | solution.py:277
  4.7 31.8 %collective-permute-start.2 = (bf16[256,512]{1,0:T(8,128)(2,1)S(1)}, bf16[256,512]{1,0:T(8,128)(2,1)S(1)}, u32[]{:S(2)}, u32[]{:S(2)}) collective-permute-start(bf16[256,512]{1,0:T(8,128)(2,1)S(1)} %constant_dynamic-update-slice_fusion.refs_0_), channel_id=1, source_target_pairs={{0,24},{8,0},{16,8},{24,16},{1,25},{9,1},{17,9},{25,17},{2,26},{10... | collective-permute-start | bytes 786440 | tf_op jit(solution)/shard_map/ppermute | solution.py:277
  7.9 9.6 %collective-permute-start.4 = (bf16[256,512]{1,0:T(8,128)(2,1)S(1)}, bf16[256,512]{1,0:T(8,128)(2,1)S(1)}, u32[]{:S(2)}, u32[]{:S(2)}) collective-permute-start(bf16[256,512]{1,0:T(8,128)(2,1)S(1)} %constant_dynamic-update-slice_fusion.2.refs_4_), channel_id=1, source_target_pairs={{0,24},{8,0},{16,8},{24,16},{1,25},{9,1},{17,9},{25,17},{2,26},{10... | collective-permute-start | bytes 786440 | tf_op jit(solution)/shard_map/ppermute | solution.py:277
  9.3 27.1 %collective-permute-start.3 = (bf16[256,512]{1,0:T(8,128)(2,1)S(1)}, bf16[256,512]{1,0:T(8,128)(2,1)S(1)}, u32[]{:S(2)}, u32[]{:S(2)}) collective-permute-start(bf16[256,512]{1,0:T(8,128)(2,1)S(1)} %constant_dynamic-update-slice_fusion.2.refs_4_), channel_id=1, source_target_pairs={{0,8},{8,16},{16,24},{24,0},{1,9},{9,17},{17,25},{25,1},{2,10},{10... | collective-permute-start | bytes 786440 | tf_op jit(solution)/shard_map/ppermute | solution.py:277
  11.1 9.7 %all-to-all-start = ((bf16[4,256,128]{2,1,0:T(8,128)(2,1)}), bf16[4,256,128]{2,1,0:T(8,128)(2,1)S(1)}, u32[]{:S(2)}, u32[]{:S(2)}) async-start(bf16[4,256,128]{2,1,0:T(8,128)(2,1)} %bitcast.11), calls=%async_computation | async-start | bytes 524288 | tf_op jit(solution)/shard_map/all_to_all | solution.py:281
  15.9 20.5 %collective-permute-start.1 = (bf16[256,512]{1,0:T(8,128)(2,1)S(1)}, bf16[256,512]{1,0:T(8,128)(2,1)S(1)}, u32[]{:S(2)}, u32[]{:S(2)}) collective-permute-start(bf16[256,512]{1,0:T(8,128)(2,1)S(1)} %collective-permute-done.refs_1_), channel_id=1, source_target_pairs={{0,8},{8,16},{16,24},{24,0},{1,9},{9,17},{17,25},{25,1},{2,10},{10... | collective-permute-start | bytes 786440 | tf_op jit(solution)/shard_map/ppermute | solution.py:277
  17.5 19.0 %collective-permute-start.5 = (bf16[256,512]{1,0:T(8,128)(2,1)S(1)}, bf16[256,512]{1,0:T(8,128)(2,1)S(1)}, u32[]{:S(2)}, u32[]{:S(2)}) collective-permute-start(bf16[256,512]{1,0:T(8,128)(2,1)S(1)} %collective-permute-done.4.refs_7_), channel_id=1, source_target_pairs={{0,24},{8,0},{16,8},{24,16},{1,25},{9,1},{17,9},{25,17},{2,26},{10... | collective-permute-start | bytes 786440 | tf_op jit(solution)/shard_map/ppermute | solution.py:277
  21.7 14.8 %all-to-all-start.1 = ((f32[8,1,256]{2,1,0:T(1,128)}), f32[8,1,256]{2,1,0:T(1,128)S(1)}, u32[]{:S(2)}, u32[]{:S(2)}) async-start(f32[8,1,256]{2,1,0:T(1,128)} %shard_map.177), calls=%async_computation.1 | async-start | bytes 16384 | tf_op jit(solution)/shard_map/all_to_all | solution.py:281
  37.9 7.0 %collective-permute-start.11 = (bf16[32,2176]{1,0:T(8,128)(2,1)S(1)}, bf16[32,2176]{1,0:T(8,128)(2,1)S(1)}, u32[]{:S(2)}, u32[]{:S(2)}) collective-permute-start(bf16[32,2176]{1,0:T(8,128)(2,1)S(1)} %get-tuple-element.16), channel_id=1, source_target_pairs={{0,224},{32,0},{64,32},{96,64},{128,96},{160,128},{192,160},{224,1... | collective-permute-start | bytes 417800 | tf_op jit(solution)/shard_map/ppermute | solution.py:277
  38.3 8.3 %collective-permute-start.10 = (bf16[32,2176]{1,0:T(8,128)(2,1)S(1)}, bf16[32,2176]{1,0:T(8,128)(2,1)S(1)}, u32[]{:S(2)}, u32[]{:S(2)}) collective-permute-start(bf16[32,2176]{1,0:T(8,128)(2,1)S(1)} %get-tuple-element.15), channel_id=1, source_target_pairs={{0,224},{32,0},{64,32},{96,64},{128,96},{160,128},{192,160},{224,1... | collective-permute-start | bytes 417800 | tf_op jit(solution)/shard_map/ppermute | solution.py:277
  39.3 14.9 %collective-permute-start.6 = (bf16[32,2176]{1,0:T(8,128)(2,1)S(1)}, bf16[32,2176]{1,0:T(8,128)(2,1)S(1)}, u32[]{:S(2)}, u32[]{:S(2)}) collective-permute-start(bf16[32,2176]{1,0:T(8,128)(2,1)S(1)} %get-tuple-element.11), channel_id=1, source_target_pairs={{0,96},{32,128},{64,160},{96,192},{128,224},{160,0},{192,32},{224,... | collective-permute-start | bytes 417800 | tf_op jit(solution)/shard_map/ppermute | solution.py:277
  41.4 12.9 %collective-permute-start.7 = (bf16[32,2176]{1,0:T(8,128)(2,1)S(1)}, bf16[32,2176]{1,0:T(8,128)(2,1)S(1)}, u32[]{:S(2)}, u32[]{:S(2)}) collective-permute-start(bf16[32,2176]{1,0:T(8,128)(2,1)S(1)} %get-tuple-element.12), channel_id=1, source_target_pairs={{0,64},{32,96},{64,128},{96,160},{128,192},{160,224},{192,0},{224,... | collective-permute-start | bytes 417800 | tf_op jit(solution)/shard_map/ppermute | solution.py:277
  42.9 11.4 %collective-permute-start.8 = (bf16[32,2176]{1,0:T(8,128)(2,1)S(1)}, bf16[32,2176]{1,0:T(8,128)(2,1)S(1)}, u32[]{:S(2)}, u32[]{:S(2)}) collective-permute-start(bf16[32,2176]{1,0:T(8,128)(2,1)S(1)} %get-tuple-element.13), channel_id=1, source_target_pairs={{0,192},{32,224},{64,0},{96,32},{128,64},{160,96},{192,128},{224,1... | collective-permute-start | bytes 417800 | tf_op jit(solution)/shard_map/ppermute | solution.py:277
  44.9 15.3 %collective-permute-start.9 = (bf16[32,2176]{1,0:T(8,128)(2,1)S(1)}, bf16[32,2176]{1,0:T(8,128)(2,1)S(1)}, u32[]{:S(2)}, u32[]{:S(2)}) collective-permute-start(bf16[32,2176]{1,0:T(8,128)(2,1)S(1)} %get-tuple-element.14), channel_id=1, source_target_pairs={{0,32},{32,64},{64,96},{96,128},{128,160},{160,192},{192,224},{224... | collective-permute-start | bytes 417800 | tf_op jit(solution)/shard_map/ppermute | solution.py:277
  46.6 13.7 %collective-permute-start.12 = (bf16[32,2176]{1,0:T(8,128)(2,1)S(1)}, bf16[32,2176]{1,0:T(8,128)(2,1)S(1)}, u32[]{:S(2)}, u32[]{:S(2)}) collective-permute-start(bf16[32,2176]{1,0:T(8,128)(2,1)S(1)} %shard_map.179), channel_id=1, source_target_pairs={{0,160},{32,192},{64,224},{96,0},{128,32},{160,64},{192,96},{224,1... | collective-permute-start | bytes 417800 | tf_op jit(solution)/shard_map/ppermute | solution.py:277
  47.7 12.6 %copy-start.1 = (f32[128]{0:T(128)S(1)}, f32[128]{0:T(128)}, u32[]{:S(2)}) copy-start(f32[128]{0:T(128)} %param.26) | copy-start | bytes 1540
  60.3 1.6 %copy-start.2 = (f32[8,4,128,128]{3,2,1,0:T(8,128)S(1)}, f32[8,4,128,128]{3,2,1,0:T(8,128)}, u32[]{:S(2)}) copy-start(f32[8,4,128,128]{3,2,1,0:T(8,128)} %shard_map.176.carried_ref) | copy-start | bytes 6291460
  61.9 6.4 %copy-start = (bf16[512,128]{1,0:T(8,128)(2,1)S(1)}, bf16[512,128]{1,0:T(8,128)(2,1)}, u32[]{:S(2)}) copy-start(bf16[512,128]{1,0:T(8,128)(2,1)} %w0.1) | copy-start | bytes 393220
  64.9 13.6 %all-to-all-start.2 = ((bf16[8,32,512]{2,1,0:T(8,128)(2,1)}), bf16[8,32,512]{2,1,0:T(8,128)(2,1)S(1)}, u32[]{:S(2)}, u32[]{:S(2)}) async-start(bf16[8,32,512]{2,1,0:T(8,128)(2,1)} %shard_map.180), calls=%async_computation.2 | async-start | bytes 524288 | tf_op jit(solution)/shard_map/all_to_all | solution.py:281
  68.3 5.1 %collective-permute-start.13 = (bf16[512,128]{1,0:T(8,128)(2,1)S(1)}, bf16[512,128]{1,0:T(8,128)(2,1)S(1)}, u32[]{:S(2)}, u32[]{:S(2)}) collective-permute-start(bf16[512,128]{1,0:T(8,128)(2,1)S(1)} %copy-done), channel_id=1, source_target_pairs={{0,8},{8,16},{16,24},{24,0},{1,9},{9,17},{17,25},{25,1},{2,10},{10... | collective-permute-start | bytes 393224 | tf_op jit(solution)/shard_map/ppermute | solution.py:277
  69.6 3.9 %collective-permute-start.15 = (bf16[512,128]{1,0:T(8,128)(2,1)S(1)}, bf16[512,128]{1,0:T(8,128)(2,1)S(1)}, u32[]{:S(2)}, u32[]{:S(2)}) collective-permute-start(bf16[512,128]{1,0:T(8,128)(2,1)S(1)} %copy-done), channel_id=1, source_target_pairs={{0,24},{8,0},{16,8},{24,16},{1,25},{9,1},{17,9},{25,17},{2,26},{10... | collective-permute-start | bytes 393224 | tf_op jit(solution)/shard_map/ppermute | solution.py:277
  73.4 5.0 %collective-permute-start.14 = (bf16[512,128]{1,0:T(8,128)(2,1)S(1)}, bf16[512,128]{1,0:T(8,128)(2,1)S(1)}, u32[]{:S(2)}, u32[]{:S(2)}) collective-permute-start(bf16[512,128]{1,0:T(8,128)(2,1)S(1)} %collective-permute-done.13.w1), channel_id=1, source_target_pairs={{0,8},{8,16},{16,24},{24,0},{1,9},{9,17},{17,25},{25,1},{2,10},{10... | collective-permute-start | bytes 393224 | tf_op jit(solution)/shard_map/ppermute | solution.py:277
where the time goes:
time: 102 us; the launch traced here: 101 us
  starting transfers between devices  35.1 us (34%)
  blocking collectives  21.8 us (21%)
  waiting for transfers between devices  19.7 us (19%)
  Pallas kernels  13.1 us (13%)
  local copies, waits for them, and re-layouts  10.7 us (10%)
    all_to_all x1, blocking collectives, exchange(): return lax.all_to_all(blocks, axes, 0, 0, tiled=True)  21.8 us
    ppermute x16, starting transfers between devices, shift(): return lax.ppermute(shard, axis, ring(step, lax.axis_size(axis)))  19.6 us
    all_to_all x3, starting transfers between devices, exchange(): return lax.all_to_all(blocks, axes, 0, 0, tiled=True)  15.5 us
    ppermute x16, waiting for transfers between devices, shift(): return lax.ppermute(shard, axis, ring(step, lax.axis_size(axis)))  13.4 us
    pallas_call x1, Pallas kernels, step(): call(carried_kernel, whole, [ANY] + [VMEM] * 4, 1 << 31, [buffer, buffer,...  6.5 us
    all_to_all x3, waiting for transfers between devices, exchange(): return lax.all_to_all(blocks, axes, 0, 0, tiled=True)  6.23 us
    unnamed x21, local copies, waits for them, and re-layouts  3.49 us
    pallas_call x1, Pallas kernels, step(): call(attend_kernel, shape((ZS, ROWS, COLS), bf16), [SMEM] + [VMEM] * 9, 1...  3.02 us
  transfers between devices with their start and end apart: 19, of which 5 were waited for; matrix products, arithmetic and copies ran while one was open for 7% of the time, Pallas kernels for 7%

commit v1 on v0

--- a/solution.py
+++ b/solution.py
@@ -77,7 +77,7 @@
     ]
 
 
-def carried_kernel(state_ref, keys_ref, values_ref, logs_ref, beta_ref, out_ref, old_ref, new_ref, sems):
+def carried_kernel(state_ref, keys_ref, values_ref, logs_ref, beta_ref, out_ref, near_ref, old_ref, new_ref, sems):
     loads = head_copies(state_ref, old_ref, sems.at[0], True)
     stores = head_copies(out_ref, new_ref, sems.at[1], False)
     for load in loads:
@@ -105,48 +105,56 @@
         for j in range(SEQ):
             step = hidot(jnp.where(lane == j, kcols, 0.0), urows)
             keep = decay[-1, last][j : j + 1, :]
-            new_ref[h, j] = keep * old_ref[h, j] + step
+            fresh = keep * old_ref[h, j] + step
+            new_ref[h, j] = fresh
+            near_ref[h, j] = fresh
         stores[h].start()
     for store in stores:
         store.wait()
 
 
-def squares_kernel(tok_ref, out_ref):
-    total = jnp.zeros((GROUP, 128), f32)
+def blocks_kernel(tok_ref, out_ref):
     for s in range(XS):
-        feats = tok_ref[s].astype(f32)
-        total = total + feats * feats
-    ones = jnp.ones((8, 128), f32)
-    rows = lax.dot_general(
-        ones, total, (((1,), (1,)), ((), ())), precision=lax.Precision.HIGHEST, preferred_element_type=f32
-    )
-    for s in range(ZS):
-        out_ref[s] = rows[0:1]
-
-
-def columns_kernel(place_ref, tok_ref, squares_ref, gain_ref, ab_ref, *refs):
-    pieces, (own_ref, *block_refs, norm_ref, scale_ref) = (refs[: 2 * XS], refs[2 * XS :])
-    z, x = (place_ref[0], place_ref[1])
-    squares = squares_ref[0]
-    for s in range(1, ZS):
-        squares = squares + squares_ref[s]
-    scale = lax.rsqrt(squares / 4096 + epsilon)
-    scale_ref[...] = jnp.broadcast_to(scale, (128, GROUP)).T
-    extra = jnp.zeros((GROUP, 16), f32)
+        for d in range(ZS):
+            out_ref[s, d * ROWS : (d + 1) * ROWS, :] = tok_ref[d, s]
+
+
+def columns_kernel(z_ref, x_ref, tp_ref, tok_ref, gain_ref, decay_ref, beta_ref, *refs):
+    pieces, (own_ref, *block_refs, high_ref, low_ref) = (refs[: 2 * XS], refs[2 * XS :])
+    z, x, tp = (z_ref[0], x_ref[0], tp_ref[0])
+    every = jnp.zeros((GROUP, 2 * HEADS * TP), f32)
+    squares = jnp.zeros((GROUP, 128), f32)
     for r in range(XS):
         at = lax.rem(x + XS - r, XS)
-        for d in range(ZS):
-            rows = pl.ds(pl.multiple_of(lax.rem(z + d, ZS) * ROWS, ROWS), ROWS)
-            feats = tok_ref[at, rows, :].astype(f32)
-            piece = (feats * scale_ref[rows, :] * gain_ref[at]).astype(bf16)
-            norm_ref[d * ROWS : (d + 1) * ROWS, r * 128 : (r + 1) * 128] = piece
-        extra = extra + lax.dot_general(
-            norm_ref[:, r * 128 : (r + 1) * 128],
-            ab_ref[at],
-            (((1,), (1,)), ((), ())),
-            preferred_element_type=f32,
-        )
-    normed = norm_ref[...]
+        gain = gain_ref[pl.ds(z * XS + at, 1), :]
+        feats = jnp.concatenate(
+            [
+                tok_ref[at, pl.ds(pl.multiple_of(lax.rem(z + d, ZS) * ROWS, ROWS), ROWS), :]
+                for d in range(ZS)
+            ],
+            axis=0,
+        ).astype(f32)
+        squares = squares + feats * feats
+        feats = feats * gain
+        high = feats.astype(bf16)
+        low = (feats - high.astype(f32)).astype(bf16)
+        high_ref[:, r * 128 : (r + 1) * 128] = high
+        low_ref[:, r * 128 : (r + 1) * 128] = low
+        lanes = pl.ds(pl.multiple_of((z * XS + at) * 128, 128), 128)
+        small = jnp.concatenate([decay_ref[:, lanes], beta_ref[:, lanes]], axis=0)
+        for part in (high, low):
+            every = every + lax.dot_general(
+                part, small, (((1,), (1,)), ((), ())), preferred_element_type=f32
+            )
+    row = lax.broadcasted_iota(jnp.int32, (2 * HEADS * TP, 16), 0)
+    col = lax.broadcasted_iota(jnp.int32, (2 * HEADS * TP, 16), 1)
+    wanted = jnp.where(col < HEADS, col, col - HEADS + HEADS * TP) + tp * HEADS
+    pick = jnp.logical_and(row == wanted, col < 2 * HEADS)
+    extra = hidot(every, jnp.where(pick, 1.0, 0.0))
+    col = lax.broadcasted_iota(jnp.int32, (GROUP, 16), 1)
+    extra = jnp.where(col == 2 * HEADS, lane_sum(squares), extra)
+    high = high_ref[...]
+    low = low_ref[...]
 
     def put(lo, hi, part):
         for d in range(ZS):
@@ -160,15 +168,17 @@
     for pair in range(2):
         mine = pieces[pair * XS : (pair + 1) * XS]
         for half in range(2):
-            weight = jnp.concatenate([w[half * 128 : (half + 1) * 128, :] for w in mine], axis=0)
+            weight = jnp.concatenate([w[:, half * COLS : (half + 1) * COLS] for w in mine], axis=0)
             at = (2 * pair + half) * COLS
-            put(at, at + COLS, jnp.dot(normed, weight, preferred_element_type=f32))
+            total = jnp.dot(high, weight, preferred_element_type=f32)
+            total = total + jnp.dot(low, weight, preferred_element_type=f32)
+            put(at, at + COLS, total)
     zero = jnp.zeros((GROUP, 112), f32)
     put(4 * COLS, WIDE, jnp.concatenate([extra, zero], axis=1))
-    low = extra - extra.astype(bf16).astype(f32)
+    rest = extra - extra.astype(bf16).astype(f32)
     for d in range(1, ZS):
         if d != FOLD:
-            rows = low[d * ROWS : (d + 1) * ROWS]
+            rows = rest[d * ROWS : (d + 1) * ROWS]
             block_refs[d - 1][:, 4 * COLS + 16 : 4 * COLS + 32] = rows.astype(bf16)
 
 
@@ -190,7 +200,7 @@
     return a * jax.nn.sigmoid(a)
 
 
-def attend_kernel(rate_ref, carried_ref, gain_ref, own_ref, *refs):
+def attend_kernel(tp_ref, rate_ref, carried_ref, gain_ref, own_ref, *refs):
     came, (out_ref, rows_ref, heads_ref) = (refs[:-3], refs[-3:])
 
     def total(lo, hi):
@@ -206,19 +216,26 @@
         )
 
     extra = regroup(0, total(4 * COLS, WIDE))
+    extra = extra[:, :16] + extra[:, 16:32]
+    scale = lax.rsqrt(extra[:, 2 * HEADS : 2 * HEADS + 1] / 4096 + epsilon)
+
+    def raw(index, lo, hi):
+        return regroup(index, total(lo, hi)) * scale
+
     for h in range(HEADS):
         lo, hi = (h * DK, (h + 1) * DK)
         spot = 1 + 4 * h
-        query = unit(silu(regroup(spot, total(lo, hi)))) * DK ** (-0.5)
-        key = unit(silu(regroup(spot + 1, total(COLS + lo, COLS + hi))))
-        value = silu(regroup(spot + 2, total(2 * COLS + lo, 2 * COLS + hi)))
-        gate = silu(regroup(spot + 3, total(3 * COLS + lo, 3 * COLS + hi)))
-        araw = extra[:, h : h + 1] + extra[:, 16 + h : 17 + h]
-        braw = extra[:, 4 + h : 5 + h] + extra[:, 20 + h : 21 + h]
+        query = unit(silu(raw(spot, lo, hi))) * DK ** (-0.5)
+        key = unit(silu(raw(spot + 1, COLS + lo, COLS + hi)))
+        value = silu(raw(spot + 2, 2 * COLS + lo, 2 * COLS + hi))
+        gate = silu(raw(spot + 3, 3 * COLS + lo, 3 * COLS + hi))
+        araw = extra[:, h : h + 1] * scale
+        braw = extra[:, HEADS + h : HEADS + h + 1] * scale
         strength = jax.nn.sigmoid(braw)
         soft = jnp.maximum(araw, 0.0) + jnp.log1p(jnp.exp(-jnp.abs(araw)))
-        log = -rate_ref[h] * soft
-        matrix = carried_ref[:, h].reshape(SEQ * DK, DK)
+        mine = lax.broadcasted_iota(jnp.int32, rate_ref.shape, 1) == tp_ref[0] * HEADS + h
+        log = -lane_sum(jnp.where(mine, rate_ref[...], 0.0)) * soft
+        matrix = carried_ref[h].reshape(SEQ * DK, DK)
         read = hidot(spread(jnp.concatenate([key, query], axis=0), SEQ), matrix)
         keys = [slab(key, t) for t in range(PROPS)]
         decay = decays([slab(log, t) for t in range(PROPS)])
@@ -261,12 +278,12 @@
         out_ref[pl.ds(s * ROWS, ROWS), :] = total.astype(bf16)
 
 
-def call(kernel, out, specs, flops, scratch=(), grant=16384, placed=VMEM):
+def call(kernel, out, specs, flops, scratch=(), grant=16384, placed=None):
     return pl.pallas_call(
         kernel,
         out_shape=out,
         in_specs=specs,
-        out_specs=jax.tree.map(lambda _: placed, out),
+        out_specs=placed or jax.tree.map(lambda _: VMEM, out),
         scratch_shapes=scratch,
         compiler_params=pltpu.CompilerParams(vmem_limit_bytes=grant * 1024),
         cost_estimate=pl.CostEstimate(flops=flops, bytes_accessed=1 << 20, transcendentals=0),
@@ -304,13 +321,15 @@
     x = lax.axis_index("x")
     tp = lax.axis_index("tp")
     shape = jax.ShapeDtypeStruct
-    xs = x.astype(jnp.int32).reshape(1)
-
-    blocks = tokens.reshape(ZS, XS, ROWS, 128).transpose(1, 0, 2, 3).reshape(XS, GROUP, 128)
+    zs, xs, tps = (i.astype(jnp.int32).reshape(1) for i in (z, x, tp))
+
+    blocks = call(blocks_kernel, shape((XS, GROUP, 128), bf16), [VMEM], 1 << 20)(
+        tokens.reshape(ZS, XS, ROWS, 128)
+    )
     tok = exchange(blocks, "x")
 
-    w_qk = jnp.concatenate([w_query, w_key], axis=0)
-    w_vz = jnp.concatenate([w_value, w_gate], axis=0)
+    w_qk = jnp.concatenate([w_query, w_key], axis=1)
+    w_vz = jnp.concatenate([w_value, w_gate], axis=1)
     qk1 = shift(w_qk, 1)
     vz3 = shift(w_vz, -1)
     vz1 = shift(w_vz, 1)
@@ -318,26 +337,17 @@
     qk2 = shift(qk1, 1)
     vz2 = shift(vz3, -1)
 
-    squares = call(squares_kernel, shape((ZS, 1, GROUP), f32), [VMEM], 1 << 20)(tok)
-    squares = exchange(squares, "z")
-    gain = lax.dynamic_slice_in_dim(norm_gain, z * 512, 512, 0).reshape(XS, 1, 128)
-    ab = jnp.concatenate(
-        [
-            lax.dynamic_slice(w.T, (tp * HEADS, z * 512), (HEADS, 512)).reshape(HEADS, XS, 128)
-            for w in (w_decay, w_beta)
-        ]
-        + [jnp.zeros((8, XS, 128), bf16)],
-        axis=0,
-    ).transpose(1, 0, 2)
-
     types = [f32 if d in (0, FOLD) else bf16 for d in range(ZS)]
     own, *block = call(
         columns_kernel,
         [shape((ROWS, WIDE), t) for t in types],
-        [SMEM] + [VMEM] * 12,
+        [SMEM] * 3 + [VMEM] * 12,
         2 * GROUP * 512 * 2048,
-        [pltpu.VMEM((GROUP, 512), bf16), pltpu.VMEM((GROUP, 128), f32)],
-    )(jnp.stack([z, x]).astype(jnp.int32), tok, squares, gain, ab, w_qk, qk1, qk2, qk3, w_vz, vz1, vz2, vz3)
+        [pltpu.VMEM((GROUP, 512), bf16)] * 2,
+    )(
+        zs, xs, tps, tok, norm_gain.reshape(ZS * XS, 128), w_decay.T, w_beta.T,
+        w_qk, qk1, qk2, qk3, w_vz, vz1, vz2, vz3,
+    )
     came = {4: shift(block[3], -1, "z")}
     for d in (3, 2, 6, 1, 7):
         came[d] = shift(block[d - 1], d, "z")
@@ -355,27 +365,26 @@
     old_values = prev_values.astype(f32).transpose(1, 2, 0, 3).reshape(HEADS, ROWS, DK)
     whole = shape(state.shape, f32)
     buffer = pltpu.VMEM((HEADS, SEQ, DK, DK), f32)
-    carried = call(
+    carried, near = call(
         carried_kernel,
-        whole,
+        (whole, shape((HEADS, SEQ, DK, DK), f32)),
         [ANY] + [VMEM] * 4,
         1 << 31,
         [buffer, buffer, pltpu.SemaphoreType.DMA((2, HEADS))],
-        60 * 1024,
-        ANY,
+        16384,
+        (ANY, VMEM),
     )(state, old_keys, old_values, logs, strengths)
 
-    rate = lax.dynamic_slice_in_dim(decay_rate, tp * HEADS, HEADS, 0)
     heads = call(
         attend_kernel,
         shape((ZS, ROWS, COLS), bf16),
-        [SMEM] + [VMEM] * 9,
+        [SMEM] + [VMEM] * 10,
         1 << 30,
         [
             pltpu.VMEM((1 + 4 * HEADS, ROWS, DK), f32),
             pltpu.VMEM((HEADS, ROWS, DK), f32),
         ],
-    )(rate, carried, head_gain.reshape(1, 128), own, *came.values())
+    )(tps, decay_rate.reshape(1, HEADS * TP), near, head_gain.reshape(1, 128), own, *came.values())
     heads = exchange(heads, "z")
     terms = call(
         project_kernel,

time: 102 us -> 92.4 us (0.906)
  local copies, waits for them, and re-layouts: 10.7 us -> 4.9 us
  starting transfers between devices: 35.1 us -> 38.4 us
  blocking collectives: 21.8 us -> 19.2 us
  waiting for transfers between devices: 19.7 us -> 17.3 us
  Pallas kernels: 13.1 us -> 11.3 us
    ppermute x16, starting transfers between devices: 19.6 us -> 29.3 us  [shift(): return lax.ppermute(shard, axis, ring(step, lax.axis_size(axis)))]
    all_to_all x3 -> x2, starting transfers between devices: 15.5 us -> 9.13 us  [exchange(): return lax.all_to_all(blocks, axes, 0, 0, tiled=True)]
    all_to_all x3 -> x2, waiting for transfers between devices: 6.23 us -> 1.79 us  [exchange(): return lax.all_to_all(blocks, axes, 0, 0, tiled=True)]
    all_to_all x1, blocking collectives: 21.8 us -> 19.2 us  [exchange(): return lax.all_to_all(blocks, axes, 0, 0, tiled=True)]
    reshape x2 -> x0, local copies, waits for them, and re-layouts: 2.48 us -> none  [the longest x1 1.67 us: step(): tokens.reshape(ZS, XS, ROWS, 128).transpose(1, 0, 2, 3)]
    ppermute x16, waiting for transfers between devices: 13.4 us -> 15.5 us  [shift(): return lax.ppermute(shard, axis, ring(step, lax.axis_size(axis)))]
    pallas_call x4, Pallas kernels: 11.9 us -> 10 us  [the longest x1 4.8 us: step(): call(carried_kernel, (whole, shape((HEADS, SEQ, DK, DK), f32)), [ANY] + [...]
    unnamed x21 -> x29, local copies, waits for them, and re-layouts: 3.49 us -> 2.89 us
  transfers between devices with their start and end apart: 19 -> 18, of which waited for: 5 -> 9; matrix products, arithmetic and copies ran while one was open for 7% -> 2% of each run, Pallas kernels for 7% -> 6%
where the time goes in v1:
time: 92.4 us; the launch traced here: 92 us
  starting transfers between devices  38.4 us (42%)
  blocking collectives  19.2 us (21%)
  waiting for transfers between devices  17.3 us (19%)
  Pallas kernels  11.3 us (12%)
  local copies, waits for them, and re-layouts  4.9 us (5%)
    ppermute x16, starting transfers between devices, shift(): return lax.ppermute(shard, axis, ring(step, lax.axis_size(axis)))  29.3 us
    all_to_all x1, blocking collectives, exchange(): return lax.all_to_all(blocks, axes, 0, 0, tiled=True)  19.2 us
    ppermute x16, waiting for transfers between devices, shift(): return lax.ppermute(shard, axis, ring(step, lax.axis_size(axis)))  15.5 us
    all_to_all x2, starting transfers between devices, exchange(): return lax.all_to_all(blocks, axes, 0, 0, tiled=True)  9.13 us
    pallas_call x1, Pallas kernels, step(): call(carried_kernel, (whole, shape((HEADS, SEQ, DK, DK), f32)), [ANY] + [...  4.8 us
    unnamed x29, local copies, waits for them, and re-layouts  2.89 us
    pallas_call x1, Pallas kernels, step(): call(attend_kernel, shape((ZS, ROWS, COLS), bf16), [SMEM] + [VMEM] * 10,...  2.67 us
    pallas_call x1, Pallas kernels, step(): call(columns_kernel, [shape((ROWS, WIDE), t) for t in types], [SMEM] * 3...  1.86 us
  transfers between devices with their start and end apart: 18, of which 9 were waited for; matrix products, arithmetic and copies ran while one was open for 2% of the time, Pallas kernels for 6%

profile of v1, /device:TPU:1, one launch (start us, length us, event | category | flops | bytes accessed | tf_op | source)
XLA Modules:
  0.0 92.0 jit_solution(9578115671586871167)
XLA Ops:
  0.7 1.0 %constant_dynamic-update-slice_fusion.1 = bf16[128,1024]{1,0:T(8,128)(2,1)S(1)} fusion(bf16[128,512]{1,0:T(8,128)(2,1)} %param.19), kind=kLoop, calls=%fused_computation.5 | loop fusion | bytes 262144
  1.7 0.9 constant_dynamic-update-slice_fusion.refs_0_
  2.6 2.1 %collective-permute-start = (bf16[128,1024]{1,0:T(8,128)(2,1)S(1)}, bf16[128,1024]{1,0:T(8,128)(2,1)S(1)}, u32[]{:S(2)}, u32[]{:S(2)}) collective-permute-start(bf16[128,1024]{1,0:T(8,128)(2,1)S(1)} %constant_dynamic-update-slice_fusion.refs_0_), channel_id=1, source_target_pairs={{0,8},{8,16},{16,24},{24,0},{1,9},{9,17},{17,25},{25,1},{2,10},{10... | collective-permute-start | bytes 786440 | tf_op jit(solution)/shard_map/ppermute | solution.py:294
  4.7 1.4 %collective-permute-start.2 = (bf16[128,1024]{1,0:T(8,128)(2,1)S(1)}, bf16[128,1024]{1,0:T(8,128)(2,1)S(1)}, u32[]{:S(2)}, u32[]{:S(2)}) collective-permute-start(bf16[128,1024]{1,0:T(8,128)(2,1)S(1)} %constant_dynamic-update-slice_fusion.refs_0_), channel_id=1, source_target_pairs={{0,24},{8,0},{16,8},{24,16},{1,25},{9,1},{17,9},{25,17},{2,26},{10... | collective-permute-start | bytes 786440 | tf_op jit(solution)/shard_map/ppermute | solution.py:294
  6.1 0.9 constant_dynamic-update-slice_fusion.3
  7.0 0.9 constant_dynamic-update-slice_fusion.2.refs_4_
  7.9 1.5 %collective-permute-start.4 = (bf16[128,1024]{1,0:T(8,128)(2,1)S(1)}, bf16[128,1024]{1,0:T(8,128)(2,1)S(1)}, u32[]{:S(2)}, u32[]{:S(2)}) collective-permute-start(bf16[128,1024]{1,0:T(8,128)(2,1)S(1)} %constant_dynamic-update-slice_fusion.2.refs_4_), channel_id=1, source_target_pairs={{0,24},{8,0},{16,8},{24,16},{1,25},{9,1},{17,9},{25,17},{2,26},{10... | collective-permute-start | bytes 786440 | tf_op jit(solution)/shard_map/ppermute | solution.py:294
  9.5 0.9 %copy-done.2 = bf16[256,4,128]{2,1,0:T(4,128)(2,1)S(1)} copy-done((bf16[256,4,128]{2,1,0:T(4,128)(2,1)S(1)}, bf16[256,4,128]{2,1,0:T(4,128)(2,1)}, u32[]{:S(2)}) %copy-start.2) | copy-done | bytes 262168
  10.4 0.7 shard_map.177
  11.1 3.9 %all-to-all-start = ((bf16[4,256,128]{2,1,0:T(8,128)(2,1)}), bf16[4,256,128]{2,1,0:T(8,128)(2,1)S(1)}, u32[]{:S(2)}, u32[]{:S(2)}) async-start(bf16[4,256,128]{2,1,0:T(8,128)(2,1)} %shard_map.177), calls=%async_computation | async-start | bytes 524288 | tf_op jit(solution)/shard_map/all_to_all | solution.py:298
  15.0 1.5 %collective-permute-start.1 = (bf16[128,1024]{1,0:T(8,128)(2,1)S(1)}, bf16[128,1024]{1,0:T(8,128)(2,1)S(1)}, u32[]{:S(2)}, u32[]{:S(2)}) collective-permute-start(bf16[128,1024]{1,0:T(8,128)(2,1)S(1)} %collective-permute-done.refs_1_), channel_id=1, source_target_pairs={{0,8},{8,16},{16,24},{24,0},{1,9},{9,17},{17,25},{25,1},{2,10},{10... | collective-permute-start | bytes 786440 | tf_op jit(solution)/shard_map/ppermute | solution.py:294
  16.9 2.0 %collective-permute-start.5 = (bf16[128,1024]{1,0:T(8,128)(2,1)S(1)}, bf16[128,1024]{1,0:T(8,128)(2,1)S(1)}, u32[]{:S(2)}, u32[]{:S(2)}) collective-permute-start(bf16[128,1024]{1,0:T(8,128)(2,1)S(1)} %collective-permute-done.4.refs_7_), channel_id=1, source_target_pairs={{0,24},{8,0},{16,8},{24,16},{1,25},{9,1},{17,9},{25,17},{2,26},{10... | collective-permute-start | bytes 786440 | tf_op jit(solution)/shard_map/ppermute | solution.py:294
  19.1 1.8 %all-to-all-done.tok_ref = bf16[4,256,128]{2,1,0:T(8,128)(2,1)S(1)} async-done(((bf16[4,256,128]{2,1,0:T(8,128)(2,1)}), bf16[4,256,128]{2,1,0:T(8,128)(2,1)S(1)}, u32[]{:S(2)}, u32[]{:S(2)}) %all-to-all-start) | async-done | bytes 262176 | tf_op jit(solution)/shard_map/all_to_all | solution.py:298
  20.9 3.1 %collective-permute-done.1.refs_2_ = bf16[128,1024]{1,0:T(8,128)(2,1)S(1)} collective-permute-done((bf16[128,1024]{1,0:T(8,128)(2,1)S(1)}, bf16[128,1024]{1,0:T(8,128)(2,1)S(1)}, u32[]{:S(2)}, u32[]{:S(2)}) %collective-permute-start.1) | collective-permute-done | bytes 262176 | tf_op jit(solution)/shard_map/ppermute | solution.py:294
  24.3 1.9 %shard_map.178 = (f32[32,2176]{1,0:T(8,128)S(1)}, bf16[32,2176]{1,0:T(8,128)(2,1)S(1)}, bf16[32,2176]{1,0:T(8,128)(2,1)S(1)}, bf16[32,2176]{1,0:T(8,128)(2,1)S(1...) custom-call(s32[1]{0:T(128)} %bitcast.10.z_ref, ...), custom_call_target="tpu_custom_call" | custom-call | flops 536870912 | bytes 1048576 | tf_op jit(solution)/shard_map/pallas_call | solution.py:341
  26.1 7.1 %collective-permute-start.11 = (bf16[32,2176]{1,0:T(8,128)(2,1)S(1)}, bf16[32,2176]{1,0:T(8,128)(2,1)S(1)}, u32[]{:S(2)}, u32[]{:S(2)}) collective-permute-start(bf16[32,2176]{1,0:T(8,128)(2,1)S(1)} %get-tuple-element.19), channel_id=1, source_target_pairs={{0,224},{32,0},{64,32},{96,64},{128,96},{160,128},{192,160},{224,1... | collective-permute-start | bytes 417800 | tf_op jit(solution)/shard_map/ppermute | solution.py:294
  33.2 0.7 collective-permute-start.10
  34.1 2.1 %collective-permute-start.7 = (bf16[32,2176]{1,0:T(8,128)(2,1)S(1)}, bf16[32,2176]{1,0:T(8,128)(2,1)S(1)}, u32[]{:S(2)}, u32[]{:S(2)}) collective-permute-start(bf16[32,2176]{1,0:T(8,128)(2,1)S(1)} %get-tuple-element.15), channel_id=1, source_target_pairs={{0,64},{32,96},{64,128},{96,160},{128,192},{160,224},{192,0},{224,... | collective-permute-start | bytes 417800 | tf_op jit(solution)/shard_map/ppermute | solution.py:294
  36.2 1.9 %collective-permute-start.8 = (bf16[32,2176]{1,0:T(8,128)(2,1)S(1)}, bf16[32,2176]{1,0:T(8,128)(2,1)S(1)}, u32[]{:S(2)}, u32[]{:S(2)}) collective-permute-start(bf16[32,2176]{1,0:T(8,128)(2,1)S(1)} %get-tuple-element.16), channel_id=1, source_target_pairs={{0,192},{32,224},{64,0},{96,32},{128,64},{160,96},{192,128},{224,1... | collective-permute-start | bytes 417800 | tf_op jit(solution)/shard_map/ppermute | solution.py:294
  38.1 0.5 collective-permute-start.9
  38.8 3.7 %collective-permute-start.12 = (bf16[32,2176]{1,0:T(8,128)(2,1)S(1)}, bf16[32,2176]{1,0:T(8,128)(2,1)S(1)}, u32[]{:S(2)}, u32[]{:S(2)}) collective-permute-start(bf16[32,2176]{1,0:T(8,128)(2,1)S(1)} %shard_map.179), channel_id=1, source_target_pairs={{0,160},{32,192},{64,224},{96,0},{128,32},{160,64},{192,96},{224,1... | collective-permute-start | bytes 417800 | tf_op jit(solution)/shard_map/ppermute | solution.py:294
  42.5 4.8 %shard_map.176 = (f32[8,4,128,128]{3,2,1,0:T(8,128)}, f32[4,8,128,128]{3,2,1,0:T(8,128)S(1)}) custom-call(f32[8,4,128,128]{3,2,1,0:T(8,128)S(1)} %copy-done.5, f32[4,32,128]{2,1,0:T(8,128)S(1)} %get-tuple-element.25.keys_ref, f32[4,32,128]{2,1,0:T(8,128)S(1)} %get-tuple-element.24.values_ref, f32[8,16]{1,0:T(8,128)S(1)} %copy.21.logs_ref, ...), custom_call_target="tpu_custom_call" | custom-call | flops 2147483648 | bytes 1048576 | tf_op jit(solution)/shard_map/pallas_call | solution.py:368
  47.3 4.8 %collective-permute-done.7.refs_1_ = bf16[32,2176]{1,0:T(8,128)(2,1)S(1)} collective-permute-done((bf16[32,2176]{1,0:T(8,128)(2,1)S(1)}, bf16[32,2176]{1,0:T(8,128)(2,1)S(1)}, u32[]{:S(2)}, u32[]{:S(2)}) %collective-permute-start.7) | collective-permute-done | bytes 139296 | tf_op jit(solution)/shard_map/ppermute | solution.py:294
  52.1 0.9 collective-permute-done.9.refs_3_
  53.0 2.7 %shard_map.180 = bf16[8,32,512]{2,1,0:T(8,128)(2,1)} custom-call(s32[1]{0:T(128)} %bitcast.1.tp_ref, f32[1,32]{1,0:T(1,128)S(1)} %bitcast.29, f32[4,8,128,128]{3,2,1,0:T(8,128)S(1)} %get-tuple-element.12.carried_ref, f32[1,128]{1,0:T(1,128)S(1)} %bitcast.30, f32[32,2176]{1,0:T(8,128)S(1)} %get-tuple-element.13.own_ref, ...), custom_call_target="tpu_custom_call" | custom-call | flops 1073741824 | bytes 1048576 | tf_op jit(solution)/shard_map/pallas_call | solution.py:378
  55.7 5.3 %all-to-all-start.1 = ((bf16[8,32,512]{2,1,0:T(8,128)(2,1)}), bf16[8,32,512]{2,1,0:T(8,128)(2,1)S(1)}, u32[]{:S(2)}, u32[]{:S(2)}) async-start(bf16[8,32,512]{2,1,0:T(8,128)(2,1)} %shard_map.180), calls=%async_computation.1 | async-start | bytes 524288 | tf_op jit(solution)/shard_map/all_to_all | solution.py:298
  61.0 3.0 %collective-permute-start.13 = (bf16[512,128]{1,0:T(8,128)(2,1)S(1)}, bf16[512,128]{1,0:T(8,128)(2,1)S(1)}, u32[]{:S(2)}, u32[]{:S(2)}) collective-permute-start(bf16[512,128]{1,0:T(8,128)(2,1)S(1)} %copy-done.3), channel_id=1, source_target_pairs={{0,8},{8,16},{16,24},{24,0},{1,9},{9,17},{17,25},{25,1},{2,10},{10... | collective-permute-start | bytes 393224 | tf_op jit(solution)/shard_map/ppermute | solution.py:294
  64.0 2.1 %collective-permute-done.13.w1 = bf16[512,128]{1,0:T(8,128)(2,1)S(1)} collective-permute-done((bf16[512,128]{1,0:T(8,128)(2,1)S(1)}, bf16[512,128]{1,0:T(8,128)(2,1)S(1)}, u32[]{:S(2)}, u32[]{:S(2)}) %collective-permute-start.13) | collective-permute-done | bytes 131104 | tf_op jit(solution)/shard_map/ppermute | solution.py:294
  66.1 1.7 %collective-permute-start.14 = (bf16[512,128]{1,0:T(8,128)(2,1)S(1)}, bf16[512,128]{1,0:T(8,128)(2,1)S(1)}, u32[]{:S(2)}, u32[]{:S(2)}) collective-permute-start(bf16[512,128]{1,0:T(8,128)(2,1)S(1)} %collective-permute-done.13.w1), channel_id=1, source_target_pairs={{0,8},{8,16},{16,24},{24,0},{1,9},{9,17},{17,25},{25,1},{2,10},{10... | collective-permute-start | bytes 393224 | tf_op jit(solution)/shard_map/ppermute | solution.py:294
  68.1 3.6 %collective-permute-done.14.w2 = bf16[512,128]{1,0:T(8,128)(2,1)S(1)} collective-permute-done((bf16[512,128]{1,0:T(8,128)(2,1)S(1)}, bf16[512,128]{1,0:T(8,128)(2,1)S(1)}, u32[]{:S(2)}, u32[]{:S(2)}) %collective-permute-start.14) | collective-permute-done | bytes 131104 | tf_op jit(solution)/shard_map/ppermute | solution.py:294
  72.1 19.2 %all_to_all.15.terms_ref = bf16[32,32,128]{2,1,0:T(8,128)(2,1)S(1)} all-to-all(bf16[32,32,128]{2,1,0:T(8,128)(2,1)S(1)} %shard_map.181), channel_id=1, replica_groups=mesh['z'=8,'x'=4,'tp'=8] {'x','tp'}, dimensions={0} | all-to-all | bytes 524288 | tf_op jit(solution)/shard_map/all_to_all | solution.py:298
  91.3 0.7 shard_map.182
  (50 shorter events, 2.0 us)
Async XLA Ops:
  0.6 14.3 %copy-start.12 = (s32[8]{0:T(128)S(1)}, s32[8]{0:T(128)}, u32[]{:S(2)}) copy-start(s32[8]{0:T(128)} %param.33) | copy-start | bytes 100
  0.6 14.3 %copy-start.8 = (bf16[8,4,4,128]{3,2,1,0:T(4,128)(2,1)S(1)}, bf16[8,4,4,128]{3,2,1,0:T(4,128)(2,1)}, u32[]{:S(2)}) copy-start(bf16[8,4,4,128]{3,2,1,0:T(4,128)(2,1)} %param.30) | copy-start | bytes 98308
  0.7 18.2 %copy-start.10 = (f32[8,4,4]{0,2,1:T(4,128)S(1)}, f32[8,4,4]{0,2,1:T(4,128)}, u32[]{:S(2)}) copy-start(f32[8,4,4]{0,2,1:T(4,128)} %param.32) | copy-start | bytes 1540
  0.7 18.2 %copy-start.11 = (f32[8,4,4]{0,2,1:T(4,128)S(1)}, f32[8,4,4]{0,2,1:T(4,128)}, u32[]{:S(2)}) copy-start(f32[8,4,4]{0,2,1:T(4,128)} %param.31) | copy-start | bytes 1540
  0.7 18.4 %copy-start.9 = (bf16[8,4,4,128]{3,2,1,0:T(4,128)(2,1)S(1)}, bf16[8,4,4,128]{3,2,1,0:T(4,128)(2,1)}, u32[]{:S(2)}) copy-start(bf16[8,4,4,128]{3,2,1,0:T(4,128)(2,1)} %param.29) | copy-start | bytes 98308
  0.7 23.6 %copy-start.4 = (f32[4096]{0:T(1024)S(1)}, f32[4096]{0:T(1024)}, u32[]{:S(2)}) copy-start(f32[4096]{0:T(1024)} %param.18) | copy-start | bytes 49156
  0.7 23.6 %copy-start = (bf16[4096,32]{0,1:T(8,128)(2,1)S(1)}, bf16[4096,32]{0,1:T(8,128)(2,1)}, u32[]{:S(2)}) copy-start(bf16[4096,32]{0,1:T(8,128)(2,1)} %param.23) | copy-start | bytes 786436
  0.7 23.6 %copy-start.1 = (bf16[4096,32]{0,1:T(8,128)(2,1)S(1)}, bf16[4096,32]{0,1:T(8,128)(2,1)}, u32[]{:S(2)}) copy-start(bf16[4096,32]{0,1:T(8,128)(2,1)} %param.24) | copy-start | bytes 786436
  2.6 12.4 %collective-permute-start = (bf16[128,1024]{1,0:T(8,128)(2,1)S(1)}, bf16[128,1024]{1,0:T(8,128)(2,1)S(1)}, u32[]{:S(2)}, u32[]{:S(2)}) collective-permute-start(bf16[128,1024]{1,0:T(8,128)(2,1)S(1)} %constant_dynamic-update-slice_fusion.refs_0_), channel_id=1, source_target_pairs={{0,8},{8,16},{16,24},{24,0},{1,9},{9,17},{17,25},{25,1},{2,10},{10... | collective-permute-start | bytes 786440 | tf_op jit(solution)/shard_map/ppermute | solution.py:294
  4.7 16.1 %collective-permute-start.2 = (bf16[128,1024]{1,0:T(8,128)(2,1)S(1)}, bf16[128,1024]{1,0:T(8,128)(2,1)S(1)}, u32[]{:S(2)}, u32[]{:S(2)}) collective-permute-start(bf16[128,1024]{1,0:T(8,128)(2,1)S(1)} %constant_dynamic-update-slice_fusion.refs_0_), channel_id=1, source_target_pairs={{0,24},{8,0},{16,8},{24,16},{1,25},{9,1},{17,9},{25,17},{2,26},{10... | collective-permute-start | bytes 786440 | tf_op jit(solution)/shard_map/ppermute | solution.py:294
  7.9 9.0 %collective-permute-start.4 = (bf16[128,1024]{1,0:T(8,128)(2,1)S(1)}, bf16[128,1024]{1,0:T(8,128)(2,1)S(1)}, u32[]{:S(2)}, u32[]{:S(2)}) collective-permute-start(bf16[128,1024]{1,0:T(8,128)(2,1)S(1)} %constant_dynamic-update-slice_fusion.2.refs_4_), channel_id=1, source_target_pairs={{0,24},{8,0},{16,8},{24,16},{1,25},{9,1},{17,9},{25,17},{2,26},{10... | collective-permute-start | bytes 786440 | tf_op jit(solution)/shard_map/ppermute | solution.py:294
  9.4 11.5 %collective-permute-start.3 = (bf16[128,1024]{1,0:T(8,128)(2,1)S(1)}, bf16[128,1024]{1,0:T(8,128)(2,1)S(1)}, u32[]{:S(2)}, u32[]{:S(2)}) collective-permute-start(bf16[128,1024]{1,0:T(8,128)(2,1)S(1)} %constant_dynamic-update-slice_fusion.2.refs_4_), channel_id=1, source_target_pairs={{0,8},{8,16},{16,24},{24,0},{1,9},{9,17},{17,25},{25,1},{2,10},{10... | collective-permute-start | bytes 786440 | tf_op jit(solution)/shard_map/ppermute | solution.py:294
  9.5 0.9 %copy-start.2 = (bf16[256,4,128]{2,1,0:T(4,128)(2,1)S(1)}, bf16[256,4,128]{2,1,0:T(4,128)(2,1)}, u32[]{:S(2)}) copy-start(bf16[256,4,128]{2,1,0:T(4,128)(2,1)} %param.17) | copy-start | bytes 786436
  11.1 9.7 %all-to-all-start = ((bf16[4,256,128]{2,1,0:T(8,128)(2,1)}), bf16[4,256,128]{2,1,0:T(8,128)(2,1)S(1)}, u32[]{:S(2)}, u32[]{:S(2)}) async-start(bf16[4,256,128]{2,1,0:T(8,128)(2,1)} %shard_map.177), calls=%async_computation | async-start | bytes 524288 | tf_op jit(solution)/shard_map/all_to_all | solution.py:298
  15.0 8.9 %collective-permute-start.1 = (bf16[128,1024]{1,0:T(8,128)(2,1)S(1)}, bf16[128,1024]{1,0:T(8,128)(2,1)S(1)}, u32[]{:S(2)}, u32[]{:S(2)}) collective-permute-start(bf16[128,1024]{1,0:T(8,128)(2,1)S(1)} %collective-permute-done.refs_1_), channel_id=1, source_target_pairs={{0,8},{8,16},{16,24},{24,0},{1,9},{9,17},{17,25},{25,1},{2,10},{10... | collective-permute-start | bytes 786440 | tf_op jit(solution)/shard_map/ppermute | solution.py:294
  16.9 7.3 %collective-permute-start.5 = (bf16[128,1024]{1,0:T(8,128)(2,1)S(1)}, bf16[128,1024]{1,0:T(8,128)(2,1)S(1)}, u32[]{:S(2)}, u32[]{:S(2)}) collective-permute-start(bf16[128,1024]{1,0:T(8,128)(2,1)S(1)} %collective-permute-done.4.refs_7_), channel_id=1, source_target_pairs={{0,24},{8,0},{16,8},{24,16},{1,25},{9,1},{17,9},{25,17},{2,26},{10... | collective-permute-start | bytes 786440 | tf_op jit(solution)/shard_map/ppermute | solution.py:294
  20.9 21.7 %copy-start.5 = (f32[8,4,128,128]{3,2,1,0:T(8,128)S(1)}, f32[8,4,128,128]{3,2,1,0:T(8,128)}, u32[]{:S(2)}) copy-start(f32[8,4,128,128]{3,2,1,0:T(8,128)} %state_ref.1) | copy-start | bytes 6291460
  26.1 12.0 %collective-permute-start.11 = (bf16[32,2176]{1,0:T(8,128)(2,1)S(1)}, bf16[32,2176]{1,0:T(8,128)(2,1)S(1)}, u32[]{:S(2)}, u32[]{:S(2)}) collective-permute-start(bf16[32,2176]{1,0:T(8,128)(2,1)S(1)} %get-tuple-element.19), channel_id=1, source_target_pairs={{0,224},{32,0},{64,32},{96,64},{128,96},{160,128},{192,160},{224,1... | collective-permute-start | bytes 417800 | tf_op jit(solution)/shard_map/ppermute | solution.py:294
  33.2 5.6 %collective-permute-start.10 = (bf16[32,2176]{1,0:T(8,128)(2,1)S(1)}, bf16[32,2176]{1,0:T(8,128)(2,1)S(1)}, u32[]{:S(2)}, u32[]{:S(2)}) collective-permute-start(bf16[32,2176]{1,0:T(8,128)(2,1)S(1)} %get-tuple-element.18), channel_id=1, source_target_pairs={{0,224},{32,0},{64,32},{96,64},{128,96},{160,128},{192,160},{224,1... | collective-permute-start | bytes 417800 | tf_op jit(solution)/shard_map/ppermute | solution.py:294
  34.0 13.3 %collective-permute-start.6 = (bf16[32,2176]{1,0:T(8,128)(2,1)S(1)}, bf16[32,2176]{1,0:T(8,128)(2,1)S(1)}, u32[]{:S(2)}, u32[]{:S(2)}) collective-permute-start(bf16[32,2176]{1,0:T(8,128)(2,1)S(1)} %get-tuple-element.14), channel_id=1, source_target_pairs={{0,96},{32,128},{64,160},{96,192},{128,224},{160,0},{192,32},{224,... | collective-permute-start | bytes 417800 | tf_op jit(solution)/shard_map/ppermute | solution.py:294
  34.1 18.0 %collective-permute-start.7 = (bf16[32,2176]{1,0:T(8,128)(2,1)S(1)}, bf16[32,2176]{1,0:T(8,128)(2,1)S(1)}, u32[]{:S(2)}, u32[]{:S(2)}) collective-permute-start(bf16[32,2176]{1,0:T(8,128)(2,1)S(1)} %get-tuple-element.15), channel_id=1, source_target_pairs={{0,64},{32,96},{64,128},{96,160},{128,192},{160,224},{192,0},{224,... | collective-permute-start | bytes 417800 | tf_op jit(solution)/shard_map/ppermute | solution.py:294
  36.2 15.9 %collective-permute-start.8 = (bf16[32,2176]{1,0:T(8,128)(2,1)S(1)}, bf16[32,2176]{1,0:T(8,128)(2,1)S(1)}, u32[]{:S(2)}, u32[]{:S(2)}) collective-permute-start(bf16[32,2176]{1,0:T(8,128)(2,1)S(1)} %get-tuple-element.16), channel_id=1, source_target_pairs={{0,192},{32,224},{64,0},{96,32},{128,64},{160,96},{192,128},{224,1... | collective-permute-start | bytes 417800 | tf_op jit(solution)/shard_map/ppermute | solution.py:294
  38.1 14.9 %collective-permute-start.9 = (bf16[32,2176]{1,0:T(8,128)(2,1)S(1)}, bf16[32,2176]{1,0:T(8,128)(2,1)S(1)}, u32[]{:S(2)}, u32[]{:S(2)}) collective-permute-start(bf16[32,2176]{1,0:T(8,128)(2,1)S(1)} %get-tuple-element.17), channel_id=1, source_target_pairs={{0,32},{32,64},{64,96},{96,128},{128,160},{160,192},{192,224},{224... | collective-permute-start | bytes 417800 | tf_op jit(solution)/shard_map/ppermute | solution.py:294
  38.8 14.2 %collective-permute-start.12 = (bf16[32,2176]{1,0:T(8,128)(2,1)S(1)}, bf16[32,2176]{1,0:T(8,128)(2,1)S(1)}, u32[]{:S(2)}, u32[]{:S(2)}) collective-permute-start(bf16[32,2176]{1,0:T(8,128)(2,1)S(1)} %shard_map.179), channel_id=1, source_target_pairs={{0,160},{32,192},{64,224},{96,0},{128,32},{160,64},{192,96},{224,1... | collective-permute-start | bytes 417800 | tf_op jit(solution)/shard_map/ppermute | solution.py:294
  42.5 10.5 %copy-start.6 = (f32[32]{0:T(128)S(1)}, f32[32]{0:T(128)}, u32[]{:S(2)}) copy-start(f32[32]{0:T(128)} %param.25) | copy-start | bytes 388
  42.5 10.5 %copy-start.7 = (f32[128]{0:T(128)S(1)}, f32[128]{0:T(128)}, u32[]{:S(2)}) copy-start(f32[128]{0:T(128)} %param.26) | copy-start | bytes 1540
  53.0 8.0 %copy-start.3 = (bf16[512,128]{1,0:T(8,128)(2,1)S(1)}, bf16[512,128]{1,0:T(8,128)(2,1)}, u32[]{:S(2)}) copy-start(bf16[512,128]{1,0:T(8,128)(2,1)} %w0.1) | copy-start | bytes 393220
  55.7 16.0 %all-to-all-start.1 = ((bf16[8,32,512]{2,1,0:T(8,128)(2,1)}), bf16[8,32,512]{2,1,0:T(8,128)(2,1)S(1)}, u32[]{:S(2)}, u32[]{:S(2)}) async-start(bf16[8,32,512]{2,1,0:T(8,128)(2,1)} %shard_map.180), calls=%async_computation.1 | async-start | bytes 524288 | tf_op jit(solution)/shard_map/all_to_all | solution.py:298
  61.0 5.1 %collective-permute-start.13 = (bf16[512,128]{1,0:T(8,128)(2,1)S(1)}, bf16[512,128]{1,0:T(8,128)(2,1)S(1)}, u32[]{:S(2)}, u32[]{:S(2)}) collective-permute-start(bf16[512,128]{1,0:T(8,128)(2,1)S(1)} %copy-done.3), channel_id=1, source_target_pairs={{0,8},{8,16},{16,24},{24,0},{1,9},{9,17},{17,25},{25,1},{2,10},{10... | collective-permute-start | bytes 393224 | tf_op jit(solution)/shard_map/ppermute | solution.py:294
  64.0 4.1 %collective-permute-start.15 = (bf16[512,128]{1,0:T(8,128)(2,1)S(1)}, bf16[512,128]{1,0:T(8,128)(2,1)S(1)}, u32[]{:S(2)}, u32[]{:S(2)}) collective-permute-start(bf16[512,128]{1,0:T(8,128)(2,1)S(1)} %copy-done.3), channel_id=1, source_target_pairs={{0,24},{8,0},{16,8},{24,16},{1,25},{9,1},{17,9},{25,17},{2,26},{10... | collective-permute-start | bytes 393224 | tf_op jit(solution)/shard_map/ppermute | solution.py:294
  66.1 5.6 %collective-permute-start.14 = (bf16[512,128]{1,0:T(8,128)(2,1)S(1)}, bf16[512,128]{1,0:T(8,128)(2,1)S(1)}, u32[]{:S(2)}, u32[]{:S(2)}) collective-permute-start(bf16[512,128]{1,0:T(8,128)(2,1)S(1)} %collective-permute-done.13.w1), channel_id=1, source_target_pairs={{0,8},{8,16},{16,24},{24,0},{1,9},{9,17},{17,25},{25,1},{2,10},{10... | collective-permute-start | bytes 393224 | tf_op jit(solution)/shard_map/ppermute | solution.py:294

commit v2 on v1

--- a/solution.py
+++ b/solution.py
@@ -77,23 +77,52 @@
     ]
 
 
-def carried_kernel(state_ref, keys_ref, values_ref, logs_ref, beta_ref, out_ref, near_ref, old_ref, new_ref, sems):
+def carried_kernel(
+    state_ref, keys_ref, values_ref, logs_ref, beta_ref, taken_ref, out_ref, near_ref, old_ref, new_ref, rows_ref, sems
+):
     loads = head_copies(state_ref, old_ref, sems.at[0], True)
     stores = head_copies(out_ref, new_ref, sems.at[1], False)
     for load in loads:
         load.start()
     lane = lax.broadcasted_iota(jnp.int32, (DK, ROWS), 1) % SEQ
+    many = HEADS * PROPS
+
+    def to_columns(rows):
+        same = lax.broadcasted_iota(jnp.int32, (many, many), 0) == lax.broadcasted_iota(
+            jnp.int32, (many, many), 1
+        )
+        return lax.dot_general(
+            rows,
+            jnp.where(same, 1.0, 0.0),
+            (((0,), (0,)), ((), ())),
+            precision=lax.Precision.HIGHEST,
+            preferred_element_type=f32,
+        )
+
+    taken = to_columns(jnp.broadcast_to(taken_ref[...].astype(f32), (many, SEQ)))
+    which = lax.broadcasted_iota(jnp.int32, (SEQ, many), 1) % PROPS
+    keep = jnp.where(which.astype(f32) < taken, 1.0, 0.0)
+    all_logs = to_columns(logs_ref[...]) * keep
+    all_strengths = to_columns(beta_ref[...]) * keep
+    rows_ref[0] = keys_ref[...].astype(f32)
+    rows_ref[1] = values_ref[...].astype(f32)
+
+    def taken_rows(index, h):
+        return jnp.concatenate(
+            [rows_ref[index, pl.ds(h * PROPS + t, SEQ, stride=many), :] for t in range(PROPS)], axis=0
+        )
+
     for h in range(HEADS):
-        raw = keys_ref[h]
+        raw = taken_rows(0, h)
         unit = raw * lax.rsqrt(lane_sum(raw * raw) + epsilon)
-        vals = values_ref[h]
+        vals = taken_rows(1, h)
         loads[h].wait()
         matrix = old_ref[h].reshape(SEQ * DK, DK)
         read = hidot(spread(unit, SEQ), matrix)
         keys = [slab(unit, t) for t in range(PROPS)]
-        col = lambda ref, t: ref[:, h * PROPS + t : h * PROPS + t + 1]
-        logs = [col(logs_ref, t) for t in range(PROPS)]
-        strength = [col(beta_ref, t) for t in range(PROPS)]
+        col = lambda a, t: a[:, h * PROPS + t : h * PROPS + t + 1]
+        logs = [col(all_logs, t) for t in range(PROPS)]
+        strength = [col(all_strengths, t) for t in range(PROPS)]
         decay = decays(logs)
         done = writes(
             keys, [slab(vals, t) for t in range(PROPS)], strength, decay, [slab(read, t) for t in range(PROPS)]
@@ -113,35 +142,42 @@
         store.wait()
 
 
-def blocks_kernel(tok_ref, out_ref):
+def blocks_kernel(x_ref, tok_ref, *out_refs):
+    for r, ref in enumerate(out_refs):
+        at = lax.rem(x_ref[0] + r, XS)
+        for d in range(ZS):
+            ref[d * ROWS : (d + 1) * ROWS, :] = tok_ref[d, at]
+
+
+def small_kernel(z_ref, gain_ref, decay_ref, beta_ref, near_gain_ref, near_ref):
     for s in range(XS):
-        for d in range(ZS):
-            out_ref[s, d * ROWS : (d + 1) * ROWS, :] = tok_ref[d, s]
-
-
-def columns_kernel(z_ref, x_ref, tp_ref, tok_ref, gain_ref, decay_ref, beta_ref, *refs):
-    pieces, (own_ref, *block_refs, high_ref, low_ref) = (refs[: 2 * XS], refs[2 * XS :])
+        at = z_ref[0] * XS + s
+        lanes = pl.ds(pl.multiple_of(at * 128, 128), 128)
+        near_gain_ref[s] = gain_ref[pl.ds(at, 1), :]
+        near_ref[s] = jnp.concatenate([decay_ref[:, lanes], beta_ref[:, lanes]], axis=0)
+
+
+def columns_kernel(z_ref, x_ref, tp_ref, gain_ref, small_ref, *refs):
+    toks, pieces, (own_ref, *block_refs, high_ref, low_ref) = (refs[:XS], refs[XS:15], refs[15:])
     z, x, tp = (z_ref[0], x_ref[0], tp_ref[0])
     every = jnp.zeros((GROUP, 2 * HEADS * TP), f32)
     squares = jnp.zeros((GROUP, 128), f32)
     for r in range(XS):
         at = lax.rem(x + XS - r, XS)
-        gain = gain_ref[pl.ds(z * XS + at, 1), :]
         feats = jnp.concatenate(
             [
-                tok_ref[at, pl.ds(pl.multiple_of(lax.rem(z + d, ZS) * ROWS, ROWS), ROWS), :]
+                toks[r][pl.ds(pl.multiple_of(lax.rem(z + d, ZS) * ROWS, ROWS), ROWS), :]
                 for d in range(ZS)
             ],
             axis=0,
         ).astype(f32)
         squares = squares + feats * feats
-        feats = feats * gain
+        feats = feats * gain_ref[at]
         high = feats.astype(bf16)
         low = (feats - high.astype(f32)).astype(bf16)
         high_ref[:, r * 128 : (r + 1) * 128] = high
         low_ref[:, r * 128 : (r + 1) * 128] = low
-        lanes = pl.ds(pl.multiple_of((z * XS + at) * 128, 128), 128)
-        small = jnp.concatenate([decay_ref[:, lanes], beta_ref[:, lanes]], axis=0)
+        small = small_ref[at]
         for part in (high, low):
             every = every + lax.dot_general(
                 part, small, (((1,), (1,)), ((), ())), preferred_element_type=f32
@@ -166,9 +202,13 @@
                 ref[:, lo:hi] = rows.astype(ref.dtype)
 
     for pair in range(2):
-        mine = pieces[pair * XS : (pair + 1) * XS]
         for half in range(2):
-            weight = jnp.concatenate([w[:, half * COLS : (half + 1) * COLS] for w in mine], axis=0)
+            cols = slice(half * COLS, (half + 1) * COLS)
+            if pair == 0:
+                mine = [pieces[0][:, cols]] + [w[...] for w in pieces[1 + 3 * half : 4 + 3 * half]]
+            else:
+                mine = [w[:, cols] for w in pieces[7:]]
+            weight = jnp.concatenate(mine, axis=0)
             at = (2 * pair + half) * COLS
             total = jnp.dot(high, weight, preferred_element_type=f32)
             total = total + jnp.dot(low, weight, preferred_element_type=f32)
@@ -323,30 +363,40 @@
     shape = jax.ShapeDtypeStruct
     zs, xs, tps = (i.astype(jnp.int32).reshape(1) for i in (z, x, tp))
 
-    blocks = call(blocks_kernel, shape((XS, GROUP, 128), bf16), [VMEM], 1 << 20)(
-        tokens.reshape(ZS, XS, ROWS, 128)
-    )
-    tok = exchange(blocks, "x")
-
-    w_qk = jnp.concatenate([w_query, w_key], axis=1)
+    t0, *away = call(
+        blocks_kernel, [shape((GROUP, 128), bf16)] * XS, [SMEM, VMEM], 1 << 20
+    )(xs, tokens.reshape(ZS, XS, ROWS, 128))
+    t1, t2, t3 = (shift(away[r - 1], r) for r in range(1, XS))
+
+    q1 = shift(w_query, 1)
+    q3 = shift(w_query, -1)
+    k1 = shift(w_key, 1)
+    k3 = shift(w_key, -1)
     w_vz = jnp.concatenate([w_value, w_gate], axis=1)
-    qk1 = shift(w_qk, 1)
     vz3 = shift(w_vz, -1)
     vz1 = shift(w_vz, 1)
-    qk3 = shift(w_qk, -1)
-    qk2 = shift(qk1, 1)
+    q2 = shift(q1, 1)
+    k2 = shift(k1, 1)
     vz2 = shift(vz3, -1)
+    w_qk = jnp.concatenate([w_query, w_key], axis=1)
+
+    gain, small = call(
+        small_kernel,
+        (shape((XS, 1, 128), f32), shape((XS, 2 * HEADS * TP, 128), bf16)),
+        [SMEM] + [VMEM] * 3,
+        1 << 10,
+    )(zs, norm_gain.reshape(ZS * XS, 128), w_decay.T, w_beta.T)
 
     types = [f32 if d in (0, FOLD) else bf16 for d in range(ZS)]
     own, *block = call(
         columns_kernel,
         [shape((ROWS, WIDE), t) for t in types],
-        [SMEM] * 3 + [VMEM] * 12,
+        [SMEM] * 3 + [VMEM] * 17,
         2 * GROUP * 512 * 2048,
         [pltpu.VMEM((GROUP, 512), bf16)] * 2,
     )(
-        zs, xs, tps, tok, norm_gain.reshape(ZS * XS, 128), w_decay.T, w_beta.T,
-        w_qk, qk1, qk2, qk3, w_vz, vz1, vz2, vz3,
+        zs, xs, tps, gain, small, t0, t1, t2, t3,
+        w_qk, q1, q2, q3, k1, k2, k3, w_vz, vz1, vz2, vz3,
     )
     came = {4: shift(block[3], -1, "z")}
     for d in (3, 2, 6, 1, 7):
@@ -358,22 +408,26 @@
     o3 = shift(w_out, -1)
     o2 = shift(o1, 1)
 
-    keep = (jnp.arange(PROPS)[None, :] < accepted[:, None]).astype(f32)[:, None, :]
-    logs = (prev_log_decay * keep).reshape(SEQ, HEADS * PROPS)
-    strengths = (prev_beta * keep).reshape(SEQ, HEADS * PROPS)
-    old_keys = prev_keys.astype(f32).transpose(1, 2, 0, 3).reshape(HEADS, ROWS, DK)
-    old_values = prev_values.astype(f32).transpose(1, 2, 0, 3).reshape(HEADS, ROWS, DK)
     whole = shape(state.shape, f32)
+    flat = (SEQ * HEADS * PROPS, DK)
+    by_sequence = lambda a: a.transpose(1, 2, 0).reshape(HEADS * PROPS, SEQ)
     buffer = pltpu.VMEM((HEADS, SEQ, DK, DK), f32)
     carried, near = call(
         carried_kernel,
         (whole, shape((HEADS, SEQ, DK, DK), f32)),
-        [ANY] + [VMEM] * 4,
+        [ANY] + [VMEM] * 5,
         1 << 31,
-        [buffer, buffer, pltpu.SemaphoreType.DMA((2, HEADS))],
+        [buffer, buffer, pltpu.VMEM((2, *flat), f32), pltpu.SemaphoreType.DMA((2, HEADS))],
         16384,
         (ANY, VMEM),
-    )(state, old_keys, old_values, logs, strengths)
+    )(
+        state,
+        prev_keys.reshape(flat),
+        prev_values.reshape(flat),
+        by_sequence(prev_log_decay),
+        by_sequence(prev_beta),
+        accepted.reshape(1, SEQ),
+    )
 
     heads = call(
         attend_kernel,

time: 92.4 us -> 99 us (1.071)
  waiting for transfers between devices: 17.3 us -> 27.7 us
  starting transfers between devices: 38.4 us -> 31.7 us
  blocking collectives: 19.2 us -> 20.7 us
  other arithmetic: 0.02 us -> 1.14 us
    ppermute x16 -> x22, waiting for transfers between devices: 15.5 us -> 27.7 us  [shift(): return lax.ppermute(shard, axis, ring(step, lax.axis_size(axis)))]
    all_to_all x2 -> x1, starting transfers between devices: 9.13 us -> 5.06 us  [exchange(): return lax.all_to_all(blocks, axes, 0, 0, tiled=True)]
    ppermute x16 -> x22, starting transfers between devices: 29.3 us -> 26.6 us  [shift(): return lax.ppermute(shard, axis, ring(step, lax.axis_size(axis)))]
    all_to_all x2 -> x1, waiting for transfers between devices: 1.79 us -> 0.01 us  [exchange(): return lax.all_to_all(blocks, axes, 0, 0, tiled=True)]
    unnamed x29 -> x27, local copies, waits for them, and re-layouts: 2.89 us -> 4.53 us
    all_to_all x1, blocking collectives: 19.2 us -> 20.7 us  [exchange(): return lax.all_to_all(blocks, axes, 0, 0, tiled=True)]
    concatenate x0 -> x1, other arithmetic: none -> 1.14 us  [step(): w_qk = jnp.concatenate([w_query, w_key], axis=1)]
  transfers between devices with their start and end apart: 18 -> 23, of which waited for: 9 -> 10; matrix products, arithmetic and copies ran while one was open for 2% -> 1% of each run, Pallas kernels for 6% -> 5%
where the time goes in v2:
time: 99 us; the launch traced here: 98.5 us
  starting transfers between devices  31.7 us (32%)
  waiting for transfers between devices  27.7 us (28%)
  blocking collectives  20.7 us (21%)
  Pallas kernels  11 us (11%)
  local copies, waits for them, and re-layouts  5.44 us (5%)
  other arithmetic  1.14 us (1%)
    ppermute x22, waiting for transfers between devices, shift(): return lax.ppermute(shard, axis, ring(step, lax.axis_size(axis)))  27.7 us
    ppermute x22, starting transfers between devices, shift(): return lax.ppermute(shard, axis, ring(step, lax.axis_size(axis)))  26.6 us
    all_to_all x1, blocking collectives, exchange(): return lax.all_to_all(blocks, axes, 0, 0, tiled=True)  20.7 us
    pallas_call x1, Pallas kernels, step(): call(carried_kernel, (whole, shape((HEADS, SEQ, DK, DK), f32)), [ANY] + [...  5.13 us
    all_to_all x1, starting transfers between devices, exchange(): return lax.all_to_all(blocks, axes, 0, 0, tiled=True)  5.06 us
    unnamed x27, local copies, waits for them, and re-layouts  4.53 us
    pallas_call x1, Pallas kernels, step(): call(attend_kernel, shape((ZS, ROWS, COLS), bf16), [SMEM] + [VMEM] * 10,...  2.74 us
  transfers between devices with their start and end apart: 23, of which 10 were waited for; matrix products, arithmetic and copies ran while one was open for 1% of the time, Pallas kernels for 5%

profile of v2, /device:TPU:1, one launch (start us, length us, event | category | flops | bytes accessed | tf_op | source)
XLA Modules:
  0.0 98.5 jit_solution(1538100273654647495)
XLA Ops:
  0.6 0.9 constant_dynamic-update-slice_fusion.1
  1.5 0.9 constant_dynamic-update-slice_fusion.refs_11_
  2.5 3.4 %collective-permute-start.10 = (bf16[128,1024]{1,0:T(8,128)(2,1)S(1)}, bf16[128,1024]{1,0:T(8,128)(2,1)S(1)}, u32[]{:S(2)}, u32[]{:S(2)}) collective-permute-start(bf16[128,1024]{1,0:T(8,128)(2,1)S(1)} %constant_dynamic-update-slice_fusion.refs_11_), channel_id=1, source_target_pairs={{0,24},{8,0},{16,8},{24,16},{1,25},{9,1},{17,9},{25,17},{2,26},{10... | collective-permute-start | bytes 786440 | tf_op jit(solution)/shard_map/ppermute | solution.py:334
  5.8 0.9 copy-done.2
  6.9 1.7 %collective-permute-start.1 = (bf16[256,128]{1,0:T(8,128)(2,1)S(1)}, bf16[256,128]{1,0:T(8,128)(2,1)S(1)}, u32[]{:S(2)}, u32[]{:S(2)}) collective-permute-start(bf16[256,128]{1,0:T(8,128)(2,1)S(1)} %get-tuple-element.23), channel_id=1, source_target_pairs={{0,16},{8,24},{16,0},{24,8},{1,17},{9,25},{17,1},{25,9},{2,18},{10... | collective-permute-start | bytes 196616 | tf_op jit(solution)/shard_map/ppermute | solution.py:334
  8.7 0.9 collective-permute-start.2
  10.2 1.4 %collective-permute-done.refs_1_ = bf16[256,128]{1,0:T(8,128)(2,1)S(1)} collective-permute-done((bf16[256,128]{1,0:T(8,128)(2,1)S(1)}, bf16[256,128]{1,0:T(8,128)(2,1)S(1)}, u32[]{:S(2)}, u32[]{:S(2)}) %collective-permute-start) | collective-permute-done | bytes 65568 | tf_op jit(solution)/shard_map/ppermute | solution.py:334
  12.3 1.5 %collective-permute-start.6 = (bf16[128,512]{1,0:T(8,128)(2,1)}, bf16[128,512]{1,0:T(8,128)(2,1)S(1)}, u32[]{:S(2)}, u32[]{:S(2)}) collective-permute-start(bf16[128,512]{1,0:T(8,128)(2,1)} %param.20), channel_id=1, source_target_pairs={{0,8},{8,16},{16,24},{24,0},{1,9},{9,17},{17,25},{25,1},{2,10},{10... | collective-permute-start | bytes 393224 | tf_op jit(solution)/shard_map/ppermute | solution.py:334
  13.8 3.2 %collective-permute-start.5 = (bf16[128,512]{1,0:T(8,128)(2,1)}, bf16[128,512]{1,0:T(8,128)(2,1)S(1)}, u32[]{:S(2)}, u32[]{:S(2)}) collective-permute-start(bf16[128,512]{1,0:T(8,128)(2,1)} %param.19), channel_id=1, source_target_pairs={{0,24},{8,0},{16,8},{24,16},{1,25},{9,1},{17,9},{25,17},{2,26},{10... | collective-permute-start | bytes 393224 | tf_op jit(solution)/shard_map/ppermute | solution.py:334
  17.1 3.8 %collective-permute-done.3.refs_5_ = bf16[128,512]{1,0:T(8,128)(2,1)S(1)} collective-permute-done((bf16[128,512]{1,0:T(8,128)(2,1)}, bf16[128,512]{1,0:T(8,128)(2,1)S(1)}, u32[]{:S(2)}, u32[]{:S(2)}) %collective-permute-start.3) | collective-permute-done | bytes 131104 | tf_op jit(solution)/shard_map/ppermute | solution.py:334
  21.0 2.7 %collective-permute-done.6.refs_8_ = bf16[128,512]{1,0:T(8,128)(2,1)S(1)} collective-permute-done((bf16[128,512]{1,0:T(8,128)(2,1)}, bf16[128,512]{1,0:T(8,128)(2,1)S(1)}, u32[]{:S(2)}, u32[]{:S(2)}) %collective-permute-start.6) | collective-permute-done | bytes 131104 | tf_op jit(solution)/shard_map/ppermute | solution.py:334
  23.7 0.9 collective-permute-start.7
  24.6 0.9 copy-done
  25.6 0.9 copy-done.1
  26.5 0.7 copy-done.4
  27.3 1.1 %pad_maximum_fusion.refs_4_ = bf16[128,1024]{1,0:T(8,128)(2,1)S(1)} fusion(bf16[128,512]{1,0:T(8,128)(2,1)} %param.20, bf16[128,512]{1,0:T(8,128)(2,1)} %param.19), kind=kLoop, calls=%fused_computation | loop fusion | flops 524288 | bytes 524288 | tf_op jit(solution)/shard_map/concatenate | solution.py:381
  28.7 1.9 %collective-permute-done.7.refs_9_ = bf16[128,512]{1,0:T(8,128)(2,1)S(1)} collective-permute-done((bf16[128,512]{1,0:T(8,128)(2,1)S(1)}, bf16[128,512]{1,0:T(8,128)(2,1)S(1)}, u32[]{:S(2)}, u32[]{:S(2)}) %collective-permute-start.7) | collective-permute-done | bytes 131104 | tf_op jit(solution)/shard_map/ppermute | solution.py:334
  30.6 1.8 %shard_map.179 = (f32[32,2176]{1,0:T(8,128)S(1)}, bf16[32,2176]{1,0:T(8,128)(2,1)S(1)}, bf16[32,2176]{1,0:T(8,128)(2,1)S(1)}, bf16[32,2176]{1,0:T(8,128)(2,1)S(1...) custom-call(s32[1]{0:T(128)} %bitcast.11.z_ref, ...), custom_call_target="tpu_custom_call" | custom-call | flops 536870912 | bytes 1048576 | tf_op jit(solution)/shard_map/pallas_call | solution.py:391
  32.4 5.1 %collective-permute-start.17 = (bf16[32,2176]{1,0:T(8,128)(2,1)S(1)}, bf16[32,2176]{1,0:T(8,128)(2,1)S(1)}, u32[]{:S(2)}, u32[]{:S(2)}) collective-permute-start(bf16[32,2176]{1,0:T(8,128)(2,1)S(1)} %get-tuple-element.31), channel_id=1, source_target_pairs={{0,224},{32,0},{64,32},{96,64},{128,96},{160,128},{192,160},{224,1... | collective-permute-start | bytes 417800 | tf_op jit(solution)/shard_map/ppermute | solution.py:334
  37.5 2.8 %collective-permute-start.13 = (bf16[32,2176]{1,0:T(8,128)(2,1)S(1)}, bf16[32,2176]{1,0:T(8,128)(2,1)S(1)}, u32[]{:S(2)}, u32[]{:S(2)}) collective-permute-start(bf16[32,2176]{1,0:T(8,128)(2,1)S(1)} %get-tuple-element.27), channel_id=1, source_target_pairs={{0,64},{32,96},{64,128},{96,160},{128,192},{160,224},{192,0},{224,... | collective-permute-start | bytes 417800 | tf_op jit(solution)/shard_map/ppermute | solution.py:334
  40.3 0.8 collective-permute-start.14
  41.1 1.9 %collective-permute-start.15 = (bf16[32,2176]{1,0:T(8,128)(2,1)S(1)}, bf16[32,2176]{1,0:T(8,128)(2,1)S(1)}, u32[]{:S(2)}, u32[]{:S(2)}) collective-permute-start(bf16[32,2176]{1,0:T(8,128)(2,1)S(1)} %get-tuple-element.29), channel_id=1, source_target_pairs={{0,32},{32,64},{64,96},{96,128},{128,160},{160,192},{192,224},{224... | collective-permute-start | bytes 417800 | tf_op jit(solution)/shard_map/ppermute | solution.py:334
  43.0 0.8 collective-permute-start.16
  43.9 6.6 %collective-permute-done.12.refs_0_ = bf16[32,2176]{1,0:T(8,128)(2,1)S(1)} collective-permute-done((bf16[32,2176]{1,0:T(8,128)(2,1)S(1)}, bf16[32,2176]{1,0:T(8,128)(2,1)S(1)}, u32[]{:S(2)}, u32[]{:S(2)}) %collective-permute-start.12) | collective-permute-done | bytes 139296 | tf_op jit(solution)/shard_map/ppermute | solution.py:334
  50.6 5.1 %shard_map.176 = (f32[8,4,128,128]{3,2,1,0:T(8,128)}, f32[4,8,128,128]{3,2,1,0:T(8,128)S(1)}) custom-call(f32[8,4,128,128]{3,2,1,0:T(8,128)S(1)} %copy-done.5, bf16[128,128]{1,0:T(8,128)(2,1)S(1)} %bitcast.23, bf16[128,128]{1,0:T(8,128)(2,1)S(1)} %bitcast.24, f32[16,8]{1,0:T(8,128)S(1)} %bitcast.25, f32[16,8]{1,0:T(8,128)S(1)} %bitcast.26, s32[1,8]{1,0:T(1,128)S(1)} %bitcast.27), custom_call_target="tpu_custom_call" | custom-call | flops 2147483648 | bytes 1048576 | tf_op jit(solution)/shard_map/pallas_call | solution.py:415
  55.8 2.1 %collective-permute-done.18.refs_5_ = bf16[32,2176]{1,0:T(8,128)(2,1)S(1)} collective-permute-done((bf16[32,2176]{1,0:T(8,128)(2,1)S(1)}, bf16[32,2176]{1,0:T(8,128)(2,1)S(1)}, u32[]{:S(2)}, u32[]{:S(2)}) %collective-permute-start.18) | collective-permute-done | bytes 139296 | tf_op jit(solution)/shard_map/ppermute | solution.py:334
  57.8 2.7 %shard_map.181 = bf16[8,32,512]{2,1,0:T(8,128)(2,1)} custom-call(s32[1]{0:T(128)} %bitcast.1.tp_ref, f32[1,32]{1,0:T(1,128)S(1)} %bitcast.28, f32[4,8,128,128]{3,2,1,0:T(8,128)S(1)} %get-tuple-element.18.carried_ref, f32[1,128]{1,0:T(1,128)S(1)} %bitcast.29, f32[32,2176]{1,0:T(8,128)S(1)} %get-tuple-element.25.own_ref, ...), custom_call_target="tpu_custom_call" | custom-call | flops 1073741824 | bytes 1048576 | tf_op jit(solution)/shard_map/pallas_call | solution.py:432
  60.6 5.1 %all-to-all-start = ((bf16[8,32,512]{2,1,0:T(8,128)(2,1)}), bf16[8,32,512]{2,1,0:T(8,128)(2,1)S(1)}, u32[]{:S(2)}, u32[]{:S(2)}) async-start(bf16[8,32,512]{2,1,0:T(8,128)(2,1)} %shard_map.181), calls=%async_computation | async-start | bytes 524288 | tf_op jit(solution)/shard_map/all_to_all | solution.py:338
  65.7 2.7 %collective-permute-start.21 = (bf16[512,128]{1,0:T(8,128)(2,1)S(1)}, bf16[512,128]{1,0:T(8,128)(2,1)S(1)}, u32[]{:S(2)}, u32[]{:S(2)}) collective-permute-start(bf16[512,128]{1,0:T(8,128)(2,1)S(1)} %copy-done.3), channel_id=1, source_target_pairs={{0,24},{8,0},{16,8},{24,16},{1,25},{9,1},{17,9},{25,17},{2,26},{10... | collective-permute-start | bytes 393224 | tf_op jit(solution)/shard_map/ppermute | solution.py:334
  68.4 2.4 %collective-permute-done.19.w1 = bf16[512,128]{1,0:T(8,128)(2,1)S(1)} collective-permute-done((bf16[512,128]{1,0:T(8,128)(2,1)S(1)}, bf16[512,128]{1,0:T(8,128)(2,1)S(1)}, u32[]{:S(2)}, u32[]{:S(2)}) %collective-permute-start.19) | collective-permute-done | bytes 131104 | tf_op jit(solution)/shard_map/ppermute | solution.py:334
  70.8 5.9 %collective-permute-done.20.w2 = bf16[512,128]{1,0:T(8,128)(2,1)S(1)} collective-permute-done((bf16[512,128]{1,0:T(8,128)(2,1)S(1)}, bf16[512,128]{1,0:T(8,128)(2,1)S(1)}, u32[]{:S(2)}, u32[]{:S(2)}) %collective-permute-start.20) | collective-permute-done | bytes 131104 | tf_op jit(solution)/shard_map/ppermute | solution.py:334
  77.1 20.7 %all_to_all.10.terms_ref = bf16[32,32,128]{2,1,0:T(8,128)(2,1)S(1)} all-to-all(bf16[32,32,128]{2,1,0:T(8,128)(2,1)S(1)} %shard_map.182), channel_id=1, replica_groups=mesh['z'=8,'x'=4,'tp'=8] {'x','tp'}, dimensions={0} | all-to-all | bytes 524288 | tf_op jit(solution)/shard_map/all_to_all | solution.py:338
  (52 shorter events, 3.2 us)
Async XLA Ops:
  2.5 14.6 %collective-permute-start.10 = (bf16[128,1024]{1,0:T(8,128)(2,1)S(1)}, bf16[128,1024]{1,0:T(8,128)(2,1)S(1)}, u32[]{:S(2)}, u32[]{:S(2)}) collective-permute-start(bf16[128,1024]{1,0:T(8,128)(2,1)S(1)} %constant_dynamic-update-slice_fusion.refs_11_), channel_id=1, source_target_pairs={{0,24},{8,0},{16,8},{24,16},{1,25},{9,1},{17,9},{25,17},{2,26},{10... | collective-permute-start | bytes 786440 | tf_op jit(solution)/shard_map/ppermute | solution.py:334
  6.8 43.7 %copy-start.6 = (bf16[8,4,4,128]{3,2,1,0:T(4,128)(2,1)S(1)}, bf16[8,4,4,128]{3,2,1,0:T(4,128)(2,1)}, u32[]{:S(2)}) copy-start(bf16[8,4,4,128]{3,2,1,0:T(4,128)(2,1)} %param.29) | copy-start | bytes 98308
  6.8 43.7 %copy-start.7 = (bf16[8,4,4,128]{3,2,1,0:T(4,128)(2,1)S(1)}, bf16[8,4,4,128]{3,2,1,0:T(4,128)(2,1)}, u32[]{:S(2)}) copy-start(bf16[8,4,4,128]{3,2,1,0:T(4,128)(2,1)} %param.30) | copy-start | bytes 98308
  6.8 43.7 %copy-start.8 = (f32[8,4,4]{0,2,1:T(4,128)S(1)}, f32[8,4,4]{0,2,1:T(4,128)}, u32[]{:S(2)}) copy-start(f32[8,4,4]{0,2,1:T(4,128)} %param.31) | copy-start | bytes 1540
  6.8 43.7 %copy-start.9 = (f32[8,4,4]{0,2,1:T(4,128)S(1)}, f32[8,4,4]{0,2,1:T(4,128)}, u32[]{:S(2)}) copy-start(f32[8,4,4]{0,2,1:T(4,128)} %param.32) | copy-start | bytes 1540
  6.8 43.7 %copy-start.10 = (s32[8]{0:T(128)S(1)}, s32[8]{0:T(128)}, u32[]{:S(2)}) copy-start(s32[8]{0:T(128)} %param.33) | copy-start | bytes 100
  6.9 4.8 %collective-permute-start = (bf16[256,128]{1,0:T(8,128)(2,1)S(1)}, bf16[256,128]{1,0:T(8,128)(2,1)S(1)}, u32[]{:S(2)}, u32[]{:S(2)}) collective-permute-start(bf16[256,128]{1,0:T(8,128)(2,1)S(1)} %get-tuple-element.22), channel_id=1, source_target_pairs={{0,8},{8,16},{16,24},{24,0},{1,9},{9,17},{17,25},{25,1},{2,10},{10... | collective-permute-start | bytes 196616 | tf_op jit(solution)/shard_map/ppermute | solution.py:334
  6.9 5.3 %collective-permute-start.1 = (bf16[256,128]{1,0:T(8,128)(2,1)S(1)}, bf16[256,128]{1,0:T(8,128)(2,1)S(1)}, u32[]{:S(2)}, u32[]{:S(2)}) collective-permute-start(bf16[256,128]{1,0:T(8,128)(2,1)S(1)} %get-tuple-element.23), channel_id=1, source_target_pairs={{0,16},{8,24},{16,0},{24,8},{1,17},{9,25},{17,1},{25,9},{2,18},{10... | collective-permute-start | bytes 196616 | tf_op jit(solution)/shard_map/ppermute | solution.py:334
  8.7 5.1 %collective-permute-start.2 = (bf16[256,128]{1,0:T(8,128)(2,1)S(1)}, bf16[256,128]{1,0:T(8,128)(2,1)S(1)}, u32[]{:S(2)}, u32[]{:S(2)}) collective-permute-start(bf16[256,128]{1,0:T(8,128)(2,1)S(1)} %get-tuple-element.24), channel_id=1, source_target_pairs={{0,24},{8,0},{16,8},{24,16},{1,25},{9,1},{17,9},{25,17},{2,26},{10... | collective-permute-start | bytes 196616 | tf_op jit(solution)/shard_map/ppermute | solution.py:334
  9.6 18.8 %collective-permute-start.9 = (bf16[128,1024]{1,0:T(8,128)(2,1)S(1)}, bf16[128,1024]{1,0:T(8,128)(2,1)S(1)}, u32[]{:S(2)}, u32[]{:S(2)}) collective-permute-start(bf16[128,1024]{1,0:T(8,128)(2,1)S(1)} %constant_dynamic-update-slice_fusion.refs_11_), channel_id=1, source_target_pairs={{0,8},{8,16},{16,24},{24,0},{1,9},{9,17},{17,25},{25,1},{2,10},{10... | collective-permute-start | bytes 786440 | tf_op jit(solution)/shard_map/ppermute | solution.py:334
  11.6 9.2 %collective-permute-start.3 = (bf16[128,512]{1,0:T(8,128)(2,1)}, bf16[128,512]{1,0:T(8,128)(2,1)S(1)}, u32[]{:S(2)}, u32[]{:S(2)}) collective-permute-start(bf16[128,512]{1,0:T(8,128)(2,1)} %param.19), channel_id=1, source_target_pairs={{0,8},{8,16},{16,24},{24,0},{1,9},{9,17},{17,25},{25,1},{2,10},{10... | collective-permute-start | bytes 393224 | tf_op jit(solution)/shard_map/ppermute | solution.py:334
  12.3 11.4 %collective-permute-start.6 = (bf16[128,512]{1,0:T(8,128)(2,1)}, bf16[128,512]{1,0:T(8,128)(2,1)S(1)}, u32[]{:S(2)}, u32[]{:S(2)}) collective-permute-start(bf16[128,512]{1,0:T(8,128)(2,1)} %param.20), channel_id=1, source_target_pairs={{0,8},{8,16},{16,24},{24,0},{1,9},{9,17},{17,25},{25,1},{2,10},{10... | collective-permute-start | bytes 393224 | tf_op jit(solution)/shard_map/ppermute | solution.py:334
  13.8 9.9 %collective-permute-start.5 = (bf16[128,512]{1,0:T(8,128)(2,1)}, bf16[128,512]{1,0:T(8,128)(2,1)S(1)}, u32[]{:S(2)}, u32[]{:S(2)}) collective-permute-start(bf16[128,512]{1,0:T(8,128)(2,1)} %param.19), channel_id=1, source_target_pairs={{0,24},{8,0},{16,8},{24,16},{1,25},{9,1},{17,9},{25,17},{2,26},{10... | collective-permute-start | bytes 393224 | tf_op jit(solution)/shard_map/ppermute | solution.py:334
  17.1 13.5 %collective-permute-start.11 = (bf16[128,1024]{1,0:T(8,128)(2,1)S(1)}, bf16[128,1024]{1,0:T(8,128)(2,1)S(1)}, u32[]{:S(2)}, u32[]{:S(2)}) collective-permute-start(bf16[128,1024]{1,0:T(8,128)(2,1)S(1)} %collective-permute-done.10.refs_14_), channel_id=1, source_target_pairs={{0,24},{8,0},{16,8},{24,16},{1,25},{9,1},{17,9},{25,17},{2,26},{10... | collective-permute-start | bytes 786440 | tf_op jit(solution)/shard_map/ppermute | solution.py:334
  20.9 7.6 %collective-permute-start.8 = (bf16[128,512]{1,0:T(8,128)(2,1)}, bf16[128,512]{1,0:T(8,128)(2,1)S(1)}, u32[]{:S(2)}, u32[]{:S(2)}) collective-permute-start(bf16[128,512]{1,0:T(8,128)(2,1)} %param.20), channel_id=1, source_target_pairs={{0,24},{8,0},{16,8},{24,16},{1,25},{9,1},{17,9},{25,17},{2,26},{10... | collective-permute-start | bytes 393224 | tf_op jit(solution)/shard_map/ppermute | solution.py:334
  23.7 5.0 %collective-permute-start.4 = (bf16[128,512]{1,0:T(8,128)(2,1)S(1)}, bf16[128,512]{1,0:T(8,128)(2,1)S(1)}, u32[]{:S(2)}, u32[]{:S(2)}) collective-permute-start(bf16[128,512]{1,0:T(8,128)(2,1)S(1)} %collective-permute-done.3.refs_5_), channel_id=1, source_target_pairs={{0,8},{8,16},{16,24},{24,0},{1,9},{9,17},{17,25},{25,1},{2,10},{10... | collective-permute-start | bytes 393224 | tf_op jit(solution)/shard_map/ppermute | solution.py:334
  23.7 6.9 %collective-permute-start.7 = (bf16[128,512]{1,0:T(8,128)(2,1)S(1)}, bf16[128,512]{1,0:T(8,128)(2,1)S(1)}, u32[]{:S(2)}, u32[]{:S(2)}) collective-permute-start(bf16[128,512]{1,0:T(8,128)(2,1)S(1)} %collective-permute-done.6.refs_8_), channel_id=1, source_target_pairs={{0,8},{8,16},{16,24},{24,0},{1,9},{9,17},{17,25},{25,1},{2,10},{10... | collective-permute-start | bytes 393224 | tf_op jit(solution)/shard_map/ppermute | solution.py:334
  27.3 23.3 %copy-start.5 = (f32[8,4,128,128]{3,2,1,0:T(8,128)S(1)}, f32[8,4,128,128]{3,2,1,0:T(8,128)}, u32[]{:S(2)}) copy-start(f32[8,4,128,128]{3,2,1,0:T(8,128)} %state_ref.1) | copy-start | bytes 6291460
  32.4 10.5 %collective-permute-start.17 = (bf16[32,2176]{1,0:T(8,128)(2,1)S(1)}, bf16[32,2176]{1,0:T(8,128)(2,1)S(1)}, u32[]{:S(2)}, u32[]{:S(2)}) collective-permute-start(bf16[32,2176]{1,0:T(8,128)(2,1)S(1)} %get-tuple-element.31), channel_id=1, source_target_pairs={{0,224},{32,0},{64,32},{96,64},{128,96},{160,128},{192,160},{224,1... | collective-permute-start | bytes 417800 | tf_op jit(solution)/shard_map/ppermute | solution.py:334
  37.5 13.0 %collective-permute-start.12 = (bf16[32,2176]{1,0:T(8,128)(2,1)S(1)}, bf16[32,2176]{1,0:T(8,128)(2,1)S(1)}, u32[]{:S(2)}, u32[]{:S(2)}) collective-permute-start(bf16[32,2176]{1,0:T(8,128)(2,1)S(1)} %get-tuple-element.26), channel_id=1, source_target_pairs={{0,96},{32,128},{64,160},{96,192},{128,224},{160,0},{192,32},{224,... | collective-permute-start | bytes 417800 | tf_op jit(solution)/shard_map/ppermute | solution.py:334
  37.5 18.2 %collective-permute-start.13 = (bf16[32,2176]{1,0:T(8,128)(2,1)S(1)}, bf16[32,2176]{1,0:T(8,128)(2,1)S(1)}, u32[]{:S(2)}, u32[]{:S(2)}) collective-permute-start(bf16[32,2176]{1,0:T(8,128)(2,1)S(1)} %get-tuple-element.27), channel_id=1, source_target_pairs={{0,64},{32,96},{64,128},{96,160},{128,192},{160,224},{192,0},{224,... | collective-permute-start | bytes 417800 | tf_op jit(solution)/shard_map/ppermute | solution.py:334
  40.3 15.5 %collective-permute-start.14 = (bf16[32,2176]{1,0:T(8,128)(2,1)S(1)}, bf16[32,2176]{1,0:T(8,128)(2,1)S(1)}, u32[]{:S(2)}, u32[]{:S(2)}) collective-permute-start(bf16[32,2176]{1,0:T(8,128)(2,1)S(1)} %get-tuple-element.28), channel_id=1, source_target_pairs={{0,192},{32,224},{64,0},{96,32},{128,64},{160,96},{192,128},{224,1... | collective-permute-start | bytes 417800 | tf_op jit(solution)/shard_map/ppermute | solution.py:334
  41.1 14.7 %collective-permute-start.15 = (bf16[32,2176]{1,0:T(8,128)(2,1)S(1)}, bf16[32,2176]{1,0:T(8,128)(2,1)S(1)}, u32[]{:S(2)}, u32[]{:S(2)}) collective-permute-start(bf16[32,2176]{1,0:T(8,128)(2,1)S(1)} %get-tuple-element.29), channel_id=1, source_target_pairs={{0,32},{32,64},{64,96},{96,128},{128,160},{160,192},{192,224},{224... | collective-permute-start | bytes 417800 | tf_op jit(solution)/shard_map/ppermute | solution.py:334
  43.0 12.8 %collective-permute-start.16 = (bf16[32,2176]{1,0:T(8,128)(2,1)S(1)}, bf16[32,2176]{1,0:T(8,128)(2,1)S(1)}, u32[]{:S(2)}, u32[]{:S(2)}) collective-permute-start(bf16[32,2176]{1,0:T(8,128)(2,1)S(1)} %get-tuple-element.30), channel_id=1, source_target_pairs={{0,224},{32,0},{64,32},{96,64},{128,96},{160,128},{192,160},{224,1... | collective-permute-start | bytes 417800 | tf_op jit(solution)/shard_map/ppermute | solution.py:334
  50.5 7.3 %collective-permute-start.18 = (bf16[32,2176]{1,0:T(8,128)(2,1)S(1)}, bf16[32,2176]{1,0:T(8,128)(2,1)S(1)}, u32[]{:S(2)}, u32[]{:S(2)}) collective-permute-start(bf16[32,2176]{1,0:T(8,128)(2,1)S(1)} %shard_map.180), channel_id=1, source_target_pairs={{0,160},{32,192},{64,224},{96,0},{128,32},{160,64},{192,96},{224,1... | collective-permute-start | bytes 417800 | tf_op jit(solution)/shard_map/ppermute | solution.py:334
  50.6 7.3 %copy-start.11 = (f32[32]{0:T(128)S(1)}, f32[32]{0:T(128)}, u32[]{:S(2)}) copy-start(f32[32]{0:T(128)} %param.25) | copy-start | bytes 388
  50.6 7.3 %copy-start.12 = (f32[128]{0:T(128)S(1)}, f32[128]{0:T(128)}, u32[]{:S(2)}) copy-start(f32[128]{0:T(128)} %param.26) | copy-start | bytes 1540
  57.8 7.8 %copy-start.3 = (bf16[512,128]{1,0:T(8,128)(2,1)S(1)}, bf16[512,128]{1,0:T(8,128)(2,1)}, u32[]{:S(2)}) copy-start(bf16[512,128]{1,0:T(8,128)(2,1)} %w0.1) | copy-start | bytes 393220
  60.6 16.1 %all-to-all-start = ((bf16[8,32,512]{2,1,0:T(8,128)(2,1)}), bf16[8,32,512]{2,1,0:T(8,128)(2,1)S(1)}, u32[]{:S(2)}, u32[]{:S(2)}) async-start(bf16[8,32,512]{2,1,0:T(8,128)(2,1)} %shard_map.181), calls=%async_computation | async-start | bytes 524288 | tf_op jit(solution)/shard_map/all_to_all | solution.py:338
  65.7 5.1 %collective-permute-start.19 = (bf16[512,128]{1,0:T(8,128)(2,1)S(1)}, bf16[512,128]{1,0:T(8,128)(2,1)S(1)}, u32[]{:S(2)}, u32[]{:S(2)}) collective-permute-start(bf16[512,128]{1,0:T(8,128)(2,1)S(1)} %copy-done.3), channel_id=1, source_target_pairs={{0,8},{8,16},{16,24},{24,0},{1,9},{9,17},{17,25},{25,1},{2,10},{10... | collective-permute-start | bytes 393224 | tf_op jit(solution)/shard_map/ppermute | solution.py:334
  65.7 5.0 %collective-permute-start.21 = (bf16[512,128]{1,0:T(8,128)(2,1)S(1)}, bf16[512,128]{1,0:T(8,128)(2,1)S(1)}, u32[]{:S(2)}, u32[]{:S(2)}) collective-permute-start(bf16[512,128]{1,0:T(8,128)(2,1)S(1)} %copy-done.3), channel_id=1, source_target_pairs={{0,24},{8,0},{16,8},{24,16},{1,25},{9,1},{17,9},{25,17},{2,26},{10... | collective-permute-start | bytes 393224 | tf_op jit(solution)/shard_map/ppermute | solution.py:334
  70.8 5.9 %collective-permute-start.20 = (bf16[512,128]{1,0:T(8,128)(2,1)S(1)}, bf16[512,128]{1,0:T(8,128)(2,1)S(1)}, u32[]{:S(2)}, u32[]{:S(2)}) collective-permute-start(bf16[512,128]{1,0:T(8,128)(2,1)S(1)} %collective-permute-done.19.w1), channel_id=1, source_target_pairs={{0,8},{8,16},{16,24},{24,0},{1,9},{9,17},{17,25},{25,1},{2,10},{10... | collective-permute-start | bytes 393224 | tf_op jit(solution)/shard_map/ppermute | solution.py:334
  (4 other events, 3.6 us)

commit v3 on v2

--- a/solution.py
+++ b/solution.py
@@ -36,6 +36,17 @@
     )
 
 
+def halves(a):
+    high = a.astype(bf16)
+    return high, (a - high.astype(f32)).astype(bf16)
+
+
+def neardot(a, b):
+    (ah, al), (bh, bl) = (halves(a), halves(b))
+    dot = lambda u, v: jnp.dot(u, v, preferred_element_type=f32)
+    return dot(ah, bh) + dot(ah, bl) + dot(al, bh)
+
+
 def spread(rows, matrix_count):
     which = lax.broadcasted_iota(jnp.int32, rows.shape, 0) % matrix_count
     return jnp.concatenate([jnp.where(which == j, rows, 0.0) for j in range(matrix_count)], axis=1)
@@ -118,7 +129,7 @@
         vals = taken_rows(1, h)
         loads[h].wait()
         matrix = old_ref[h].reshape(SEQ * DK, DK)
-        read = hidot(spread(unit, SEQ), matrix)
+        read = neardot(spread(unit, SEQ), matrix)
         keys = [slab(unit, t) for t in range(PROPS)]
         col = lambda a, t: a[:, h * PROPS + t : h * PROPS + t + 1]
         logs = [col(all_logs, t) for t in range(PROPS)]
@@ -131,10 +142,10 @@
         scaled = [keys[t] if t == last else decay[t, last] * keys[t] for t in range(PROPS)]
         kcols = jnp.concatenate(scaled, axis=0).T
         urows = jnp.concatenate(done, axis=0)
+        step = neardot(jnp.concatenate([jnp.where(lane == j, kcols, 0.0) for j in range(SEQ)], axis=0), urows)
         for j in range(SEQ):
-            step = hidot(jnp.where(lane == j, kcols, 0.0), urows)
             keep = decay[-1, last][j : j + 1, :]
-            fresh = keep * old_ref[h, j] + step
+            fresh = keep * old_ref[h, j] + step[j * DK : (j + 1) * DK]
             new_ref[h, j] = fresh
             near_ref[h, j] = fresh
         stores[h].start()
@@ -276,7 +287,7 @@
         mine = lax.broadcasted_iota(jnp.int32, rate_ref.shape, 1) == tp_ref[0] * HEADS + h
         log = -lane_sum(jnp.where(mine, rate_ref[...], 0.0)) * soft
         matrix = carried_ref[h].reshape(SEQ * DK, DK)
-        read = hidot(spread(jnp.concatenate([key, query], axis=0), SEQ), matrix)
+        read = neardot(spread(jnp.concatenate([key, query], axis=0), SEQ), matrix)
         keys = [slab(key, t) for t in range(PROPS)]
         decay = decays([slab(log, t) for t in range(PROPS)])
         done = writes(

time: 99 us -> 98.8 us (level)
  transfers between devices with their start and end apart: 23 -> 23, of which waited for: 10 -> 11; matrix products, arithmetic and copies ran while one was open for 1% -> 1% of each run, Pallas kernels for 5% -> 5%
where the time goes in v3:
time: 98.8 us; the launch traced here: 98.4 us
  starting transfers between devices  31.7 us (32%)
  waiting for transfers between devices  28.1 us (28%)
  blocking collectives  20.7 us (21%)
  Pallas kernels  10.5 us (11%)
  local copies, waits for them, and re-layouts  5.44 us (6%)
  other arithmetic  1.14 us (1%)
    ppermute x22, waiting for transfers between devices, shift(): return lax.ppermute(shard, axis, ring(step, lax.axis_size(axis)))  28.1 us
    ppermute x22, starting transfers between devices, shift(): return lax.ppermute(shard, axis, ring(step, lax.axis_size(axis)))  26.6 us
    all_to_all x1, blocking collectives, exchange(): return lax.all_to_all(blocks, axes, 0, 0, tiled=True)  20.7 us
    all_to_all x1, starting transfers between devices, exchange(): return lax.all_to_all(blocks, axes, 0, 0, tiled=True)  5.07 us
    pallas_call x1, Pallas kernels, step(): call(carried_kernel, (whole, shape((HEADS, SEQ, DK, DK), f32)), [ANY] + [...  4.76 us
    unnamed x27, local copies, waits for them, and re-layouts  4.53 us
    pallas_call x1, Pallas kernels, step(): call(attend_kernel, shape((ZS, ROWS, COLS), bf16), [SMEM] + [VMEM] * 10,...  2.59 us
  transfers between devices with their start and end apart: 23, of which 11 were waited for; matrix products, arithmetic and copies ran while one was open for 1% of the time, Pallas kernels for 5%

profile of v3, /device:TPU:1, one launch (start us, length us, event | category | flops | bytes accessed | tf_op | source)
XLA Modules:
  0.0 98.4 jit_solution(16982144033987630476)
XLA Ops:
  0.6 0.9 constant_dynamic-update-slice_fusion.1
  1.5 0.9 constant_dynamic-update-slice_fusion.refs_11_
  2.5 3.4 %collective-permute-start.10 = (bf16[128,1024]{1,0:T(8,128)(2,1)S(1)}, bf16[128,1024]{1,0:T(8,128)(2,1)S(1)}, u32[]{:S(2)}, u32[]{:S(2)}) collective-permute-start(bf16[128,1024]{1,0:T(8,128)(2,1)S(1)} %constant_dynamic-update-slice_fusion.refs_11_), channel_id=1, source_target_pairs={{0,24},{8,0},{16,8},{24,16},{1,25},{9,1},{17,9},{25,17},{2,26},{10... | collective-permute-start | bytes 786440 | tf_op jit(solution)/shard_map/ppermute | solution.py:345
  5.8 0.9 copy-done.2
  6.9 1.7 %collective-permute-start.1 = (bf16[256,128]{1,0:T(8,128)(2,1)S(1)}, bf16[256,128]{1,0:T(8,128)(2,1)S(1)}, u32[]{:S(2)}, u32[]{:S(2)}) collective-permute-start(bf16[256,128]{1,0:T(8,128)(2,1)S(1)} %get-tuple-element.23), channel_id=1, source_target_pairs={{0,16},{8,24},{16,0},{24,8},{1,17},{9,25},{17,1},{25,9},{2,18},{10... | collective-permute-start | bytes 196616 | tf_op jit(solution)/shard_map/ppermute | solution.py:345
  8.7 0.9 collective-permute-start.2
  10.2 1.4 %collective-permute-done.refs_1_ = bf16[256,128]{1,0:T(8,128)(2,1)S(1)} collective-permute-done((bf16[256,128]{1,0:T(8,128)(2,1)S(1)}, bf16[256,128]{1,0:T(8,128)(2,1)S(1)}, u32[]{:S(2)}, u32[]{:S(2)}) %collective-permute-start) | collective-permute-done | bytes 65568 | tf_op jit(solution)/shard_map/ppermute | solution.py:345
  12.3 1.5 %collective-permute-start.6 = (bf16[128,512]{1,0:T(8,128)(2,1)}, bf16[128,512]{1,0:T(8,128)(2,1)S(1)}, u32[]{:S(2)}, u32[]{:S(2)}) collective-permute-start(bf16[128,512]{1,0:T(8,128)(2,1)} %param.20), channel_id=1, source_target_pairs={{0,8},{8,16},{16,24},{24,0},{1,9},{9,17},{17,25},{25,1},{2,10},{10... | collective-permute-start | bytes 393224 | tf_op jit(solution)/shard_map/ppermute | solution.py:345
  13.8 3.2 %collective-permute-start.5 = (bf16[128,512]{1,0:T(8,128)(2,1)}, bf16[128,512]{1,0:T(8,128)(2,1)S(1)}, u32[]{:S(2)}, u32[]{:S(2)}) collective-permute-start(bf16[128,512]{1,0:T(8,128)(2,1)} %param.19), channel_id=1, source_target_pairs={{0,24},{8,0},{16,8},{24,16},{1,25},{9,1},{17,9},{25,17},{2,26},{10... | collective-permute-start | bytes 393224 | tf_op jit(solution)/shard_map/ppermute | solution.py:345
  17.1 3.8 %collective-permute-done.3.refs_5_ = bf16[128,512]{1,0:T(8,128)(2,1)S(1)} collective-permute-done((bf16[128,512]{1,0:T(8,128)(2,1)}, bf16[128,512]{1,0:T(8,128)(2,1)S(1)}, u32[]{:S(2)}, u32[]{:S(2)}) %collective-permute-start.3) | collective-permute-done | bytes 131104 | tf_op jit(solution)/shard_map/ppermute | solution.py:345
  21.0 2.7 %collective-permute-done.6.refs_8_ = bf16[128,512]{1,0:T(8,128)(2,1)S(1)} collective-permute-done((bf16[128,512]{1,0:T(8,128)(2,1)}, bf16[128,512]{1,0:T(8,128)(2,1)S(1)}, u32[]{:S(2)}, u32[]{:S(2)}) %collective-permute-start.6) | collective-permute-done | bytes 131104 | tf_op jit(solution)/shard_map/ppermute | solution.py:345
  23.7 0.9 collective-permute-start.7
  24.6 0.9 copy-done
  25.6 0.9 copy-done.1
  26.5 0.7 copy-done.4
  27.3 1.1 %pad_maximum_fusion.refs_4_ = bf16[128,1024]{1,0:T(8,128)(2,1)S(1)} fusion(bf16[128,512]{1,0:T(8,128)(2,1)} %param.20, bf16[128,512]{1,0:T(8,128)(2,1)} %param.19), kind=kLoop, calls=%fused_computation | loop fusion | flops 524288 | bytes 524288 | tf_op jit(solution)/shard_map/concatenate | solution.py:392
  28.7 1.9 %collective-permute-done.7.refs_9_ = bf16[128,512]{1,0:T(8,128)(2,1)S(1)} collective-permute-done((bf16[128,512]{1,0:T(8,128)(2,1)S(1)}, bf16[128,512]{1,0:T(8,128)(2,1)S(1)}, u32[]{:S(2)}, u32[]{:S(2)}) %collective-permute-start.7) | collective-permute-done | bytes 131104 | tf_op jit(solution)/shard_map/ppermute | solution.py:345
  30.6 1.8 %shard_map.179 = (f32[32,2176]{1,0:T(8,128)S(1)}, bf16[32,2176]{1,0:T(8,128)(2,1)S(1)}, bf16[32,2176]{1,0:T(8,128)(2,1)S(1)}, bf16[32,2176]{1,0:T(8,128)(2,1)S(1...) custom-call(s32[1]{0:T(128)} %bitcast.11.z_ref, ...), custom_call_target="tpu_custom_call" | custom-call | flops 536870912 | bytes 1048576 | tf_op jit(solution)/shard_map/pallas_call | solution.py:402
  32.4 5.1 %collective-permute-start.17 = (bf16[32,2176]{1,0:T(8,128)(2,1)S(1)}, bf16[32,2176]{1,0:T(8,128)(2,1)S(1)}, u32[]{:S(2)}, u32[]{:S(2)}) collective-permute-start(bf16[32,2176]{1,0:T(8,128)(2,1)S(1)} %get-tuple-element.31), channel_id=1, source_target_pairs={{0,224},{32,0},{64,32},{96,64},{128,96},{160,128},{192,160},{224,1... | collective-permute-start | bytes 417800 | tf_op jit(solution)/shard_map/ppermute | solution.py:345
  37.5 2.8 %collective-permute-start.13 = (bf16[32,2176]{1,0:T(8,128)(2,1)S(1)}, bf16[32,2176]{1,0:T(8,128)(2,1)S(1)}, u32[]{:S(2)}, u32[]{:S(2)}) collective-permute-start(bf16[32,2176]{1,0:T(8,128)(2,1)S(1)} %get-tuple-element.27), channel_id=1, source_target_pairs={{0,64},{32,96},{64,128},{96,160},{128,192},{160,224},{192,0},{224,... | collective-permute-start | bytes 417800 | tf_op jit(solution)/shard_map/ppermute | solution.py:345
  40.3 0.8 collective-permute-start.14
  41.1 1.9 %collective-permute-start.15 = (bf16[32,2176]{1,0:T(8,128)(2,1)S(1)}, bf16[32,2176]{1,0:T(8,128)(2,1)S(1)}, u32[]{:S(2)}, u32[]{:S(2)}) collective-permute-start(bf16[32,2176]{1,0:T(8,128)(2,1)S(1)} %get-tuple-element.29), channel_id=1, source_target_pairs={{0,32},{32,64},{64,96},{96,128},{128,160},{160,192},{192,224},{224... | collective-permute-start | bytes 417800 | tf_op jit(solution)/shard_map/ppermute | solution.py:345
  43.0 0.8 collective-permute-start.16
  43.9 6.6 %collective-permute-done.12.refs_0_ = bf16[32,2176]{1,0:T(8,128)(2,1)S(1)} collective-permute-done((bf16[32,2176]{1,0:T(8,128)(2,1)S(1)}, bf16[32,2176]{1,0:T(8,128)(2,1)S(1)}, u32[]{:S(2)}, u32[]{:S(2)}) %collective-permute-start.12) | collective-permute-done | bytes 139296 | tf_op jit(solution)/shard_map/ppermute | solution.py:345
  50.6 4.8 %shard_map.176 = (f32[8,4,128,128]{3,2,1,0:T(8,128)}, f32[4,8,128,128]{3,2,1,0:T(8,128)S(1)}) custom-call(f32[8,4,128,128]{3,2,1,0:T(8,128)S(1)} %copy-done.5, bf16[128,128]{1,0:T(8,128)(2,1)S(1)} %bitcast.23, bf16[128,128]{1,0:T(8,128)(2,1)S(1)} %bitcast.24, f32[16,8]{1,0:T(8,128)S(1)} %bitcast.25, f32[16,8]{1,0:T(8,128)S(1)} %bitcast.26, s32[1,8]{1,0:T(1,128)S(1)} %bitcast.27), custom_call_target="tpu_custom_call" | custom-call | flops 2147483648 | bytes 1048576 | tf_op jit(solution)/shard_map/pallas_call | solution.py:426
  55.5 2.3 %collective-permute-done.18.refs_5_ = bf16[32,2176]{1,0:T(8,128)(2,1)S(1)} collective-permute-done((bf16[32,2176]{1,0:T(8,128)(2,1)S(1)}, bf16[32,2176]{1,0:T(8,128)(2,1)S(1)}, u32[]{:S(2)}, u32[]{:S(2)}) %collective-permute-start.18) | collective-permute-done | bytes 139296 | tf_op jit(solution)/shard_map/ppermute | solution.py:345
  57.8 2.6 %shard_map.181 = bf16[8,32,512]{2,1,0:T(8,128)(2,1)} custom-call(s32[1]{0:T(128)} %bitcast.1.tp_ref, f32[1,32]{1,0:T(1,128)S(1)} %bitcast.28, f32[4,8,128,128]{3,2,1,0:T(8,128)S(1)} %get-tuple-element.18.carried_ref, f32[1,128]{1,0:T(1,128)S(1)} %bitcast.29, f32[32,2176]{1,0:T(8,128)S(1)} %get-tuple-element.25.own_ref, ...), custom_call_target="tpu_custom_call" | custom-call | flops 1073741824 | bytes 1048576 | tf_op jit(solution)/shard_map/pallas_call | solution.py:443
  60.4 5.1 %all-to-all-start = ((bf16[8,32,512]{2,1,0:T(8,128)(2,1)}), bf16[8,32,512]{2,1,0:T(8,128)(2,1)S(1)}, u32[]{:S(2)}, u32[]{:S(2)}) async-start(bf16[8,32,512]{2,1,0:T(8,128)(2,1)} %shard_map.181), calls=%async_computation | async-start | bytes 524288 | tf_op jit(solution)/shard_map/all_to_all | solution.py:349
  65.6 2.7 %collective-permute-start.21 = (bf16[512,128]{1,0:T(8,128)(2,1)S(1)}, bf16[512,128]{1,0:T(8,128)(2,1)S(1)}, u32[]{:S(2)}, u32[]{:S(2)}) collective-permute-start(bf16[512,128]{1,0:T(8,128)(2,1)S(1)} %copy-done.3), channel_id=1, source_target_pairs={{0,24},{8,0},{16,8},{24,16},{1,25},{9,1},{17,9},{25,17},{2,26},{10... | collective-permute-start | bytes 393224 | tf_op jit(solution)/shard_map/ppermute | solution.py:345
  68.3 2.4 %collective-permute-done.19.w1 = bf16[512,128]{1,0:T(8,128)(2,1)S(1)} collective-permute-done((bf16[512,128]{1,0:T(8,128)(2,1)S(1)}, bf16[512,128]{1,0:T(8,128)(2,1)S(1)}, u32[]{:S(2)}, u32[]{:S(2)}) %collective-permute-start.19) | collective-permute-done | bytes 131104 | tf_op jit(solution)/shard_map/ppermute | solution.py:345
  70.6 5.9 %collective-permute-done.20.w2 = bf16[512,128]{1,0:T(8,128)(2,1)S(1)} collective-permute-done((bf16[512,128]{1,0:T(8,128)(2,1)S(1)}, bf16[512,128]{1,0:T(8,128)(2,1)S(1)}, u32[]{:S(2)}, u32[]{:S(2)}) %collective-permute-start.20) | collective-permute-done | bytes 131104 | tf_op jit(solution)/shard_map/ppermute | solution.py:345
  77.0 20.7 %all_to_all.10.terms_ref = bf16[32,32,128]{2,1,0:T(8,128)(2,1)S(1)} all-to-all(bf16[32,32,128]{2,1,0:T(8,128)(2,1)S(1)} %shard_map.182), channel_id=1, replica_groups=mesh['z'=8,'x'=4,'tp'=8] {'x','tp'}, dimensions={0} | all-to-all | bytes 524288 | tf_op jit(solution)/shard_map/all_to_all | solution.py:349
  (52 shorter events, 3.3 us)
Async XLA Ops:
  2.5 14.6 %collective-permute-start.10 = (bf16[128,1024]{1,0:T(8,128)(2,1)S(1)}, bf16[128,1024]{1,0:T(8,128)(2,1)S(1)}, u32[]{:S(2)}, u32[]{:S(2)}) collective-permute-start(bf16[128,1024]{1,0:T(8,128)(2,1)S(1)} %constant_dynamic-update-slice_fusion.refs_11_), channel_id=1, source_target_pairs={{0,24},{8,0},{16,8},{24,16},{1,25},{9,1},{17,9},{25,17},{2,26},{10... | collective-permute-start | bytes 786440 | tf_op jit(solution)/shard_map/ppermute | solution.py:345
  6.8 43.7 %copy-start.6 = (bf16[8,4,4,128]{3,2,1,0:T(4,128)(2,1)S(1)}, bf16[8,4,4,128]{3,2,1,0:T(4,128)(2,1)}, u32[]{:S(2)}) copy-start(bf16[8,4,4,128]{3,2,1,0:T(4,128)(2,1)} %param.29) | copy-start | bytes 98308
  6.8 43.7 %copy-start.7 = (bf16[8,4,4,128]{3,2,1,0:T(4,128)(2,1)S(1)}, bf16[8,4,4,128]{3,2,1,0:T(4,128)(2,1)}, u32[]{:S(2)}) copy-start(bf16[8,4,4,128]{3,2,1,0:T(4,128)(2,1)} %param.30) | copy-start | bytes 98308
  6.8 43.7 %copy-start.8 = (f32[8,4,4]{0,2,1:T(4,128)S(1)}, f32[8,4,4]{0,2,1:T(4,128)}, u32[]{:S(2)}) copy-start(f32[8,4,4]{0,2,1:T(4,128)} %param.31) | copy-start | bytes 1540
  6.8 43.7 %copy-start.9 = (f32[8,4,4]{0,2,1:T(4,128)S(1)}, f32[8,4,4]{0,2,1:T(4,128)}, u32[]{:S(2)}) copy-start(f32[8,4,4]{0,2,1:T(4,128)} %param.32) | copy-start | bytes 1540
  6.8 43.7 %copy-start.10 = (s32[8]{0:T(128)S(1)}, s32[8]{0:T(128)}, u32[]{:S(2)}) copy-start(s32[8]{0:T(128)} %param.33) | copy-start | bytes 100
  6.9 4.8 %collective-permute-start = (bf16[256,128]{1,0:T(8,128)(2,1)S(1)}, bf16[256,128]{1,0:T(8,128)(2,1)S(1)}, u32[]{:S(2)}, u32[]{:S(2)}) collective-permute-start(bf16[256,128]{1,0:T(8,128)(2,1)S(1)} %get-tuple-element.22), channel_id=1, source_target_pairs={{0,8},{8,16},{16,24},{24,0},{1,9},{9,17},{17,25},{25,1},{2,10},{10... | collective-permute-start | bytes 196616 | tf_op jit(solution)/shard_map/ppermute | solution.py:345
  6.9 5.3 %collective-permute-start.1 = (bf16[256,128]{1,0:T(8,128)(2,1)S(1)}, bf16[256,128]{1,0:T(8,128)(2,1)S(1)}, u32[]{:S(2)}, u32[]{:S(2)}) collective-permute-start(bf16[256,128]{1,0:T(8,128)(2,1)S(1)} %get-tuple-element.23), channel_id=1, source_target_pairs={{0,16},{8,24},{16,0},{24,8},{1,17},{9,25},{17,1},{25,9},{2,18},{10... | collective-permute-start | bytes 196616 | tf_op jit(solution)/shard_map/ppermute | solution.py:345
  8.7 5.1 %collective-permute-start.2 = (bf16[256,128]{1,0:T(8,128)(2,1)S(1)}, bf16[256,128]{1,0:T(8,128)(2,1)S(1)}, u32[]{:S(2)}, u32[]{:S(2)}) collective-permute-start(bf16[256,128]{1,0:T(8,128)(2,1)S(1)} %get-tuple-element.24), channel_id=1, source_target_pairs={{0,24},{8,0},{16,8},{24,16},{1,25},{9,1},{17,9},{25,17},{2,26},{10... | collective-permute-start | bytes 196616 | tf_op jit(solution)/shard_map/ppermute | solution.py:345
  9.6 18.8 %collective-permute-start.9 = (bf16[128,1024]{1,0:T(8,128)(2,1)S(1)}, bf16[128,1024]{1,0:T(8,128)(2,1)S(1)}, u32[]{:S(2)}, u32[]{:S(2)}) collective-permute-start(bf16[128,1024]{1,0:T(8,128)(2,1)S(1)} %constant_dynamic-update-slice_fusion.refs_11_), channel_id=1, source_target_pairs={{0,8},{8,16},{16,24},{24,0},{1,9},{9,17},{17,25},{25,1},{2,10},{10... | collective-permute-start | bytes 786440 | tf_op jit(solution)/shard_map/ppermute | solution.py:345
  11.6 9.2 %collective-permute-start.3 = (bf16[128,512]{1,0:T(8,128)(2,1)}, bf16[128,512]{1,0:T(8,128)(2,1)S(1)}, u32[]{:S(2)}, u32[]{:S(2)}) collective-permute-start(bf16[128,512]{1,0:T(8,128)(2,1)} %param.19), channel_id=1, source_target_pairs={{0,8},{8,16},{16,24},{24,0},{1,9},{9,17},{17,25},{25,1},{2,10},{10... | collective-permute-start | bytes 393224 | tf_op jit(solution)/shard_map/ppermute | solution.py:345
  12.3 11.4 %collective-permute-start.6 = (bf16[128,512]{1,0:T(8,128)(2,1)}, bf16[128,512]{1,0:T(8,128)(2,1)S(1)}, u32[]{:S(2)}, u32[]{:S(2)}) collective-permute-start(bf16[128,512]{1,0:T(8,128)(2,1)} %param.20), channel_id=1, source_target_pairs={{0,8},{8,16},{16,24},{24,0},{1,9},{9,17},{17,25},{25,1},{2,10},{10... | collective-permute-start | bytes 393224 | tf_op jit(solution)/shard_map/ppermute | solution.py:345
  13.8 9.9 %collective-permute-start.5 = (bf16[128,512]{1,0:T(8,128)(2,1)}, bf16[128,512]{1,0:T(8,128)(2,1)S(1)}, u32[]{:S(2)}, u32[]{:S(2)}) collective-permute-start(bf16[128,512]{1,0:T(8,128)(2,1)} %param.19), channel_id=1, source_target_pairs={{0,24},{8,0},{16,8},{24,16},{1,25},{9,1},{17,9},{25,17},{2,26},{10... | collective-permute-start | bytes 393224 | tf_op jit(solution)/shard_map/ppermute | solution.py:345
  17.1 13.5 %collective-permute-start.11 = (bf16[128,1024]{1,0:T(8,128)(2,1)S(1)}, bf16[128,1024]{1,0:T(8,128)(2,1)S(1)}, u32[]{:S(2)}, u32[]{:S(2)}) collective-permute-start(bf16[128,1024]{1,0:T(8,128)(2,1)S(1)} %collective-permute-done.10.refs_14_), channel_id=1, source_target_pairs={{0,24},{8,0},{16,8},{24,16},{1,25},{9,1},{17,9},{25,17},{2,26},{10... | collective-permute-start | bytes 786440 | tf_op jit(solution)/shard_map/ppermute | solution.py:345
  20.9 7.6 %collective-permute-start.8 = (bf16[128,512]{1,0:T(8,128)(2,1)}, bf16[128,512]{1,0:T(8,128)(2,1)S(1)}, u32[]{:S(2)}, u32[]{:S(2)}) collective-permute-start(bf16[128,512]{1,0:T(8,128)(2,1)} %param.20), channel_id=1, source_target_pairs={{0,24},{8,0},{16,8},{24,16},{1,25},{9,1},{17,9},{25,17},{2,26},{10... | collective-permute-start | bytes 393224 | tf_op jit(solution)/shard_map/ppermute | solution.py:345
  23.7 5.0 %collective-permute-start.4 = (bf16[128,512]{1,0:T(8,128)(2,1)S(1)}, bf16[128,512]{1,0:T(8,128)(2,1)S(1)}, u32[]{:S(2)}, u32[]{:S(2)}) collective-permute-start(bf16[128,512]{1,0:T(8,128)(2,1)S(1)} %collective-permute-done.3.refs_5_), channel_id=1, source_target_pairs={{0,8},{8,16},{16,24},{24,0},{1,9},{9,17},{17,25},{25,1},{2,10},{10... | collective-permute-start | bytes 393224 | tf_op jit(solution)/shard_map/ppermute | solution.py:345
  23.7 6.9 %collective-permute-start.7 = (bf16[128,512]{1,0:T(8,128)(2,1)S(1)}, bf16[128,512]{1,0:T(8,128)(2,1)S(1)}, u32[]{:S(2)}, u32[]{:S(2)}) collective-permute-start(bf16[128,512]{1,0:T(8,128)(2,1)S(1)} %collective-permute-done.6.refs_8_), channel_id=1, source_target_pairs={{0,8},{8,16},{16,24},{24,0},{1,9},{9,17},{17,25},{25,1},{2,10},{10... | collective-permute-start | bytes 393224 | tf_op jit(solution)/shard_map/ppermute | solution.py:345
  27.3 23.3 %copy-start.5 = (f32[8,4,128,128]{3,2,1,0:T(8,128)S(1)}, f32[8,4,128,128]{3,2,1,0:T(8,128)}, u32[]{:S(2)}) copy-start(f32[8,4,128,128]{3,2,1,0:T(8,128)} %state_ref.1) | copy-start | bytes 6291460
  32.4 10.5 %collective-permute-start.17 = (bf16[32,2176]{1,0:T(8,128)(2,1)S(1)}, bf16[32,2176]{1,0:T(8,128)(2,1)S(1)}, u32[]{:S(2)}, u32[]{:S(2)}) collective-permute-start(bf16[32,2176]{1,0:T(8,128)(2,1)S(1)} %get-tuple-element.31), channel_id=1, source_target_pairs={{0,224},{32,0},{64,32},{96,64},{128,96},{160,128},{192,160},{224,1... | collective-permute-start | bytes 417800 | tf_op jit(solution)/shard_map/ppermute | solution.py:345
  37.5 13.0 %collective-permute-start.12 = (bf16[32,2176]{1,0:T(8,128)(2,1)S(1)}, bf16[32,2176]{1,0:T(8,128)(2,1)S(1)}, u32[]{:S(2)}, u32[]{:S(2)}) collective-permute-start(bf16[32,2176]{1,0:T(8,128)(2,1)S(1)} %get-tuple-element.26), channel_id=1, source_target_pairs={{0,96},{32,128},{64,160},{96,192},{128,224},{160,0},{192,32},{224,... | collective-permute-start | bytes 417800 | tf_op jit(solution)/shard_map/ppermute | solution.py:345
  37.5 17.9 %collective-permute-start.13 = (bf16[32,2176]{1,0:T(8,128)(2,1)S(1)}, bf16[32,2176]{1,0:T(8,128)(2,1)S(1)}, u32[]{:S(2)}, u32[]{:S(2)}) collective-permute-start(bf16[32,2176]{1,0:T(8,128)(2,1)S(1)} %get-tuple-element.27), channel_id=1, source_target_pairs={{0,64},{32,96},{64,128},{96,160},{128,192},{160,224},{192,0},{224,... | collective-permute-start | bytes 417800 | tf_op jit(solution)/shard_map/ppermute | solution.py:345
  40.3 15.1 %collective-permute-start.14 = (bf16[32,2176]{1,0:T(8,128)(2,1)S(1)}, bf16[32,2176]{1,0:T(8,128)(2,1)S(1)}, u32[]{:S(2)}, u32[]{:S(2)}) collective-permute-start(bf16[32,2176]{1,0:T(8,128)(2,1)S(1)} %get-tuple-element.28), channel_id=1, source_target_pairs={{0,192},{32,224},{64,0},{96,32},{128,64},{160,96},{192,128},{224,1... | collective-permute-start | bytes 417800 | tf_op jit(solution)/shard_map/ppermute | solution.py:345
  41.1 14.5 %collective-permute-start.15 = (bf16[32,2176]{1,0:T(8,128)(2,1)S(1)}, bf16[32,2176]{1,0:T(8,128)(2,1)S(1)}, u32[]{:S(2)}, u32[]{:S(2)}) collective-permute-start(bf16[32,2176]{1,0:T(8,128)(2,1)S(1)} %get-tuple-element.29), channel_id=1, source_target_pairs={{0,32},{32,64},{64,96},{96,128},{128,160},{160,192},{192,224},{224... | collective-permute-start | bytes 417800 | tf_op jit(solution)/shard_map/ppermute | solution.py:345
  43.0 12.6 %collective-permute-start.16 = (bf16[32,2176]{1,0:T(8,128)(2,1)S(1)}, bf16[32,2176]{1,0:T(8,128)(2,1)S(1)}, u32[]{:S(2)}, u32[]{:S(2)}) collective-permute-start(bf16[32,2176]{1,0:T(8,128)(2,1)S(1)} %get-tuple-element.30), channel_id=1, source_target_pairs={{0,224},{32,0},{64,32},{96,64},{128,96},{160,128},{192,160},{224,1... | collective-permute-start | bytes 417800 | tf_op jit(solution)/shard_map/ppermute | solution.py:345
  50.5 7.3 %collective-permute-start.18 = (bf16[32,2176]{1,0:T(8,128)(2,1)S(1)}, bf16[32,2176]{1,0:T(8,128)(2,1)S(1)}, u32[]{:S(2)}, u32[]{:S(2)}) collective-permute-start(bf16[32,2176]{1,0:T(8,128)(2,1)S(1)} %shard_map.180), channel_id=1, source_target_pairs={{0,160},{32,192},{64,224},{96,0},{128,32},{160,64},{192,96},{224,1... | collective-permute-start | bytes 417800 | tf_op jit(solution)/shard_map/ppermute | solution.py:345
  50.6 7.3 %copy-start.11 = (f32[32]{0:T(128)S(1)}, f32[32]{0:T(128)}, u32[]{:S(2)}) copy-start(f32[32]{0:T(128)} %param.25) | copy-start | bytes 388
  50.6 7.3 %copy-start.12 = (f32[128]{0:T(128)S(1)}, f32[128]{0:T(128)}, u32[]{:S(2)}) copy-start(f32[128]{0:T(128)} %param.26) | copy-start | bytes 1540
  57.8 7.7 %copy-start.3 = (bf16[512,128]{1,0:T(8,128)(2,1)S(1)}, bf16[512,128]{1,0:T(8,128)(2,1)}, u32[]{:S(2)}) copy-start(bf16[512,128]{1,0:T(8,128)(2,1)} %w0.1) | copy-start | bytes 393220
  60.4 16.1 %all-to-all-start = ((bf16[8,32,512]{2,1,0:T(8,128)(2,1)}), bf16[8,32,512]{2,1,0:T(8,128)(2,1)S(1)}, u32[]{:S(2)}, u32[]{:S(2)}) async-start(bf16[8,32,512]{2,1,0:T(8,128)(2,1)} %shard_map.181), calls=%async_computation | async-start | bytes 524288 | tf_op jit(solution)/shard_map/all_to_all | solution.py:349
  65.5 5.1 %collective-permute-start.19 = (bf16[512,128]{1,0:T(8,128)(2,1)S(1)}, bf16[512,128]{1,0:T(8,128)(2,1)S(1)}, u32[]{:S(2)}, u32[]{:S(2)}) collective-permute-start(bf16[512,128]{1,0:T(8,128)(2,1)S(1)} %copy-done.3), channel_id=1, source_target_pairs={{0,8},{8,16},{16,24},{24,0},{1,9},{9,17},{17,25},{25,1},{2,10},{10... | collective-permute-start | bytes 393224 | tf_op jit(solution)/shard_map/ppermute | solution.py:345
  65.6 5.0 %collective-permute-start.21 = (bf16[512,128]{1,0:T(8,128)(2,1)S(1)}, bf16[512,128]{1,0:T(8,128)(2,1)S(1)}, u32[]{:S(2)}, u32[]{:S(2)}) collective-permute-start(bf16[512,128]{1,0:T(8,128)(2,1)S(1)} %copy-done.3), channel_id=1, source_target_pairs={{0,24},{8,0},{16,8},{24,16},{1,25},{9,1},{17,9},{25,17},{2,26},{10... | collective-permute-start | bytes 393224 | tf_op jit(solution)/shard_map/ppermute | solution.py:345
  70.6 6.0 %collective-permute-start.20 = (bf16[512,128]{1,0:T(8,128)(2,1)S(1)}, bf16[512,128]{1,0:T(8,128)(2,1)S(1)}, u32[]{:S(2)}, u32[]{:S(2)}) collective-permute-start(bf16[512,128]{1,0:T(8,128)(2,1)S(1)} %collective-permute-done.19.w1), channel_id=1, source_target_pairs={{0,8},{8,16},{16,24},{24,0},{1,9},{9,17},{17,25},{25,1},{2,10},{10... | collective-permute-start | bytes 393224 | tf_op jit(solution)/shard_map/ppermute | solution.py:345
  (4 other events, 3.6 us)
